TPU v7x, 32 devices: a whole 2x2x4 slice. The times are simulated.
32 devices in a mesh: sp: 16 (over z, y, x), tp: 2 (over core).
Axes of the slice: x: 2, y: 2, z: 4, core: 2. Of those that a mesh axis runs over, the one named last changes fastest.
Arguments:
- stream_in: bfloat16 [2048, 2048], P(('sp', 'tp')), may hold values from -6 to 6
- query_compressed: bfloat16 [2048, 512], P('sp'), may hold values from -6 to 6
- keyvalue_compressed: bfloat16 [2048, 256], P('sp'), may hold values from -6 to 6
- rope_key: bfloat16 [2048, 64], P('sp'), may hold values from -153 to 153
- query_norm_gain: float32 [512], replicated, may hold values from 0.1 to 1.9
- keyvalue_norm_gain: float32 [256], replicated, may hold values from 0.1 to 1.9
- query_up_weight: bfloat16 [512, 3072], replicated, may hold values from -0.625 to 0.625
- keyvalue_up_weight: bfloat16 [256, 4096], replicated, may hold values from -0.375 to 0.375
- out_proj: bfloat16 [2048, 2048], replicated, may hold values from -0.5 to 0.5
- ffn_gain: float32 [2048], replicated, may hold values from 0.1 to 1.9
- expert_ids: int32 [2048, 4], P(('sp', 'tp')), may hold values from 0 to 15, all different within a row; in each aligned block of 64 rows (0 to 63, 64 to 127, ...) at most 32 rows name the same one
- expert_weights: float32 [2048, 4], P(('sp', 'tp')), may hold values from 0.1 to 1
- expert_gate: bfloat16 [16, 2048, 512], P('sp', None, 'tp'), may hold values from -0.125 to 0.125
- expert_up: bfloat16 [16, 2048, 512], P('sp', None, 'tp'), may hold values from -0.125 to 0.125
- expert_down: bfloat16 [16, 512, 2048], P('sp', 'tp'), may hold values from -0.25 to 0.25
- shared_gate: bfloat16 [2048, 512], replicated, may hold values from -0.125 to 0.125
- shared_up: bfloat16 [2048, 512], replicated, may hold values from -0.125 to 0.125
- shared_down: bfloat16 [512, 2048], replicated, may hold values from -0.25 to 0.25
Outputs:
- layer_out: bfloat16 [2048, 2048], P(('sp', 'tp'))
Inputs may be any that keep to these rules, and one draw needn't show every extreme that they name: `expert_ids`: each row names 4 different experts. Among the rows of one device (aligned blocks of 64 rows in token order) no expert is named by more than 32 rows, a bound that some block reaches of some device.
All inputs are finite; a program needn't handle non-finite values.
Results may differ from a plain program's by a relative error of at most 0.02.
The roundings to bfloat16 on the way count: a program that leaves them out, or rounds other values in their place, can miss the bound.
Values may be sent and summed in bfloat16 or wider, within the bound.
A program may use at most 128 MiB of HBM per device.

v0:
```python
import jax
import jax.numpy as jnp
from jax import lax
from jax.sharding import PartitionSpec as P

KEY_PLAIN_WIDTH = 128
ROTARY_WIDTH = 64
VALUE_HEAD_WIDTH = 128


epsilon = 1e-06
routed_scale = 2.5
theta_base = 10000.0


def rms_scale(values, scales):
    widened = values.astype(jnp.float32)
    inverse = lax.rsqrt(jnp.mean(widened * widened, axis=-1, keepdims=True) + epsilon)
    return widened * inverse * scales


def turn_tables(positions, rot_width):
    half_width = rot_width // 2
    frequency = theta_base ** (-(jnp.arange(half_width, dtype=jnp.float32) * 2.0) / rot_width)
    angles = positions.astype(jnp.float32)[:, None] * frequency[None, :]
    return (jnp.cos(angles), jnp.sin(angles))


def turn(values, cos_part, sine_part):
    lower_half, upper_half = jnp.split(values, 2, axis=-1)
    return jnp.concatenate(
        [
            lower_half * cos_part - upper_half * sine_part,
            upper_half * cos_part + lower_half * sine_part,
        ],
        axis=-1,
    )


def key_span(piece_rows):
    for candidate in (1024, 512, 256, 128):
        return candidate
    return piece_rows


def expand_keys(lat_block, rot_block, key_pos, keyvalue_norm_gain, keyval_cols, head_count):
    keyval_normed = rms_scale(lat_block, keyvalue_norm_gain).astype(jnp.bfloat16)
    keyvals = jnp.dot(keyval_normed, keyval_cols, preferred_element_type=jnp.float32).astype(
        jnp.bfloat16
    )
    keyvals = keyvals.reshape(lat_block.shape[0], head_count, KEY_PLAIN_WIDTH + VALUE_HEAD_WIDTH)
    cos_part, sine_part = turn_tables(key_pos, rot_block.shape[-1])
    shared_rot = turn(rot_block.astype(jnp.float32), cos_part, sine_part).astype(jnp.bfloat16)
    return (keyvals[:, :, :KEY_PLAIN_WIDTH], keyvals[:, :, KEY_PLAIN_WIDTH:], shared_rot)


def absorb(carried, queries, key_part, value_part, shared_rot):
    run_max, run_sum, run_acc = carried
    scores = jnp.einsum(
        "qhd,khd->qhk",
        queries[:, :, :KEY_PLAIN_WIDTH],
        key_part,
        preferred_element_type=jnp.float32,
    )
    scores = scores + jnp.einsum(
        "qhr,kr->qhk",
        queries[:, :, KEY_PLAIN_WIDTH:],
        shared_rot,
        preferred_element_type=jnp.float32,
    )
    new_max = jnp.maximum(run_max, jnp.max(scores, axis=-1))
    factor = jnp.exp(run_max - new_max)
    weights = jnp.exp(scores - new_max[:, :, None])
    new_sum = run_sum * factor + jnp.sum(weights, axis=-1)
    new_acc = run_acc * factor[:, :, None] + jnp.einsum(
        "qhk,khd->qhd", weights.astype(jnp.bfloat16), value_part, preferred_element_type=jnp.float32
    )
    return (new_max, new_sum, new_acc)


def attend_all(
    queries, lat_shard, rot_shard, keyvalue_norm_gain, keyval_cols, head_count, place_rows
):
    query_rows = queries.shape[0]
    initial = (
        jnp.full((query_rows, head_count), -jnp.inf, jnp.float32),
        jnp.zeros((query_rows, head_count), jnp.float32),
        jnp.zeros((query_rows, head_count, VALUE_HEAD_WIDTH), jnp.float32),
    )
    lat_piece = lax.all_gather(lat_shard, "sp", axis=0, tiled=True)
    rot_piece = lax.all_gather(rot_shard, "sp", axis=0, tiled=True)
    span_rows = key_span(lat_piece.shape[0])
    block_total = lat_piece.shape[0] // span_rows

    def one_block(inner_carried, block_index):
        lat_block = lax.dynamic_slice_in_dim(lat_piece, block_index * span_rows, span_rows, 0)
        rot_block = lax.dynamic_slice_in_dim(rot_piece, block_index * span_rows, span_rows, 0)
        key_pos = place_rows(block_index * span_rows + jnp.arange(span_rows, dtype=jnp.int32))
        key_part, value_part, shared_rot = expand_keys(
            lat_block, rot_block, key_pos, keyvalue_norm_gain, keyval_cols, head_count
        )
        return (absorb(inner_carried, queries, key_part, value_part, shared_rot), None)

    result, _ = lax.scan(one_block, initial, jnp.arange(block_total, dtype=jnp.int32))
    return result


def shards(
    stream_in,
    query_compressed,
    keyvalue_compressed,
    rope_key,
    query_norm_gain,
    keyvalue_norm_gain,
    query_up_weight,
    keyvalue_up_weight,
    out_proj,
    ffn_gain,
    expert_ids,
    expert_weights,
    expert_gate,
    expert_up,
    expert_down,
    shared_gate,
    shared_up,
    shared_down,
):
    full_gate, full_up, full_down = (
        lax.all_gather(expert_gate, "tp", axis=2, tiled=True),
        lax.all_gather(expert_up, "tp", axis=2, tiled=True),
        lax.all_gather(expert_down, "tp", axis=1, tiled=True),
    )
    tok_rows = query_compressed.shape[0]
    head_width = KEY_PLAIN_WIDTH + ROTARY_WIDTH
    pair_width = KEY_PLAIN_WIDTH + VALUE_HEAD_WIDTH
    all_heads = query_up_weight.shape[1] // head_width
    sp_index = lax.axis_index("sp")
    tp_index = lax.axis_index("tp")
    own_pos = sp_index * tok_rows + jnp.arange(tok_rows, dtype=jnp.int32)
    query_normed = rms_scale(query_compressed, query_norm_gain).astype(jnp.bfloat16)
    local_heads = all_heads // 2
    query_cols = lax.dynamic_slice_in_dim(
        query_up_weight, tp_index * local_heads * head_width, local_heads * head_width, 1
    )
    keyval_cols = lax.dynamic_slice_in_dim(
        keyvalue_up_weight, tp_index * local_heads * pair_width, local_heads * pair_width, 1
    )
    raw_query = jnp.dot(
        query_normed, query_cols, preferred_element_type=jnp.float32
    ) * head_width ** (-0.5)
    raw_query = raw_query.reshape(tok_rows, local_heads, head_width)
    cos_part, sine_part = turn_tables(own_pos, ROTARY_WIDTH)
    turned = turn(raw_query[:, :, KEY_PLAIN_WIDTH:], cos_part[:, None, :], sine_part[:, None, :])
    queries = jnp.concatenate([raw_query[:, :, :KEY_PLAIN_WIDTH], turned], axis=-1).astype(
        jnp.bfloat16
    )

    def place_whole(whole_rows):
        return whole_rows

    run_max, run_sum, run_acc = attend_all(
        queries,
        keyvalue_compressed,
        rope_key,
        keyvalue_norm_gain,
        keyval_cols,
        local_heads,
        place_whole,
    )
    local_out = (
        (run_acc / run_sum[:, :, None])
        .astype(jnp.bfloat16)
        .reshape(tok_rows, local_heads * VALUE_HEAD_WIDTH)
    )
    attended = lax.all_to_all(local_out, "tp", split_axis=0, concat_axis=1, tiled=True)
    projected = jnp.dot(attended, out_proj, preferred_element_type=jnp.float32)
    stream = (stream_in.astype(jnp.float32) + projected).astype(jnp.bfloat16)
    normed = rms_scale(stream, ffn_gain).astype(jnp.bfloat16)
    shares = (
        routed_scale * expert_weights / jnp.sum(expert_weights, axis=-1, keepdims=True)
    ).astype(jnp.bfloat16)
    moe_rows = stream_in.shape[0]
    top_count = expert_ids.shape[1]
    sp_count = lax.axis_size("sp")
    local_experts = expert_gate.shape[0]
    expert_count = local_experts * sp_count
    capacity = 2 * moe_rows * top_count // expert_count
    flat_ids = expert_ids.reshape(-1)
    hot_ids = (flat_ids[:, None] == jnp.arange(expert_count, dtype=jnp.int32)[None, :]).astype(
        jnp.int32
    )
    rank_ids = jnp.sum((jnp.cumsum(hot_ids, axis=0) - hot_ids) * hot_ids, axis=1)
    slot_ids = flat_ids * capacity + rank_ids
    hot_slots = (
        slot_ids[:, None] == jnp.arange(expert_count * capacity, dtype=jnp.int32)[None, :]
    ).reshape(moe_rows, top_count, expert_count * capacity)
    sender_map = jnp.any(hot_slots, axis=1).astype(jnp.bfloat16)
    combine = jnp.sum(jnp.where(hot_slots, shares[:, :, None], jnp.zeros((), jnp.bfloat16)), axis=1)
    outgoing = jnp.einsum(
        "ts,td->sd", sender_map, normed, preferred_element_type=jnp.float32
    ).astype(jnp.bfloat16)
    outgoing = outgoing.reshape(sp_count, local_experts, capacity, normed.shape[1])
    arrived = lax.all_to_all(outgoing, "sp", split_axis=0, concat_axis=0, tiled=True)
    gate_act = jnp.einsum("secd,edf->secf", arrived, full_gate, preferred_element_type=jnp.float32)
    up_act = jnp.einsum("secd,edf->secf", arrived, full_up, preferred_element_type=jnp.float32)
    inner_act = (jax.nn.silu(gate_act) * up_act).astype(jnp.bfloat16)
    half_hidden = inner_act.shape[-1] // 2
    first_half = jnp.einsum(
        "secf,efd->secd",
        inner_act[..., :half_hidden],
        full_down[:, :half_hidden],
        preferred_element_type=jnp.float32,
    ).astype(jnp.bfloat16)
    second_half = jnp.einsum(
        "secf,efd->secd",
        inner_act[..., half_hidden:],
        full_down[:, half_hidden:],
        preferred_element_type=jnp.float32,
    ).astype(jnp.bfloat16)
    summed = (first_half.astype(jnp.float32) + second_half.astype(jnp.float32)).astype(jnp.bfloat16)
    returned = lax.all_to_all(summed, "sp", split_axis=0, concat_axis=0, tiled=True)
    routed = jnp.dot(
        combine,
        returned.reshape(expert_count * capacity, normed.shape[1]),
        preferred_element_type=jnp.float32,
    )
    shared_inner = (
        jax.nn.silu(jnp.dot(normed, shared_gate, preferred_element_type=jnp.float32))
        * jnp.dot(normed, shared_up, preferred_element_type=jnp.float32)
    ).astype(jnp.bfloat16)
    shared_out = jnp.dot(shared_inner, shared_down, preferred_element_type=jnp.float32)
    return (stream.astype(jnp.float32) + routed + shared_out).astype(jnp.bfloat16)


def solution(mesh):
    in_specs = (
        P(("sp", "tp"), None),
        P("sp", None),
        P("sp", None),
        P("sp", None),
        P(),
        P(),
        P(),
        P(),
        P(),
        P(),
        P(("sp", "tp"), None),
        P(("sp", "tp"), None),
        P("sp", None, "tp"),
        P("sp", None, "tp"),
        P("sp", "tp", None),
        P(),
        P(),
        P(),
    )
    out_specs = P(("sp", "tp"), None)
    return jax.shard_map(shards, mesh=mesh, in_specs=in_specs, out_specs=out_specs, check_vma=False)
```

profile of v0, /device:TPU:0, one launch (start us, length us, event | category | flops | bytes accessed | tf_op | source)
XLA Modules:
  0.0 252.2 jit_solution(11174466686180340704)
XLA Ops:
  10.1 2.2 convolution_multiply_fusion
  12.3 1.4 copy.78
  14.3 46.8 %all_gather.16 = bf16[2048,64]{0,1:T(8,128)(2,1)} all-gather(bf16[128,64]{0,1:T(8,128)(2,1)S(1)} %copy-done.13), channel_id=1, replica_groups=mesh['sp'=16,'tp'=2] {'sp'}, dimensions={0}, use_global_device_ids=true | all-gather | bytes 278528 | tf_op jit(solution)/shard_map/all_gather | solution.py:91
  62.9 2.3 constant_dynamic-slice_fusion
  65.2 3.2 %all-gather.5.cloned.1.call-done = bf16[2048,256]{1,0:T(8,128)(2,1)} async-done(((bf16[128,256]{1,0:T(8,128)(2,1)}), bf16[2048,256]{1,0:T(8,128)(2,1)}) %all-gather.5.cloned.1.call-update) | async-done | bytes 1048592 | tf_op jit(solution)/shard_map/all_gather | solution.py:90
  68.4 45.4 %while.15 = (s32[]{:T(128)}, f32[128,8]{0,1:T(8,128)S(1)}, f32[128,8]{0,1:T(8,128)S(1)}, f32[128,8,128]{0,2,1:T(8,128)}, s32[2]{0:T(128)S(1)}, /*index=5*/bf16[2...) while((s32[]{:T(128)}, f32[128,8]{0,1:T(8,128)S(1)}, ...), condition=%wide.region_5.6_spmd.clone, body=%wide.region_1.5_spmd.clone.sunk | while | flops 1756078208 | bytes 72443560 | solution.py:104
  69.7 1.3 fusion.130
  70.9 2.7 %convolution_convert_fusion.5 = bf16[1024,2048]{1,0:T(8,128)(2,1)S(1)} fusion(bf16[256,2048]{1,0:T(8,128)(2,1)} %get-tuple-element.279, f32[256]{0:T(256)S(1)} %get-tuple-element.278, f32[1024]{0:T(1024)S(1)} %add_rsqrt_fusion.4, bf16[2048,256]{1,0:T(8,128)(2,1)} %get-tuple-element.277, s32[]{:T(128)S(6)} %select_n.22), kind=kOutput, calls=%fused_computation.2.clone.1 | convolution fusion | flops 1076887552 | bytes 5772292 | tf_op jit(solution)/shard_map/while/body/eval_jaxpr/dot_general | solution.py:48
  73.6 1.5 copy.110
  75.4 2.7 %fusion.132 = f32[8,1024,128]{2,1,0:T(8,128)} fusion(bf16[1024,8,128]{2,1,0:T(8,128)(2,1)S(1)} %get-tuple-element.238, bf16[128,8,192]{2,0,1:T(8,128)(2,1)S(1)} %get-tuple-element.280), kind=kOutput, calls=%fused_computation.7.clone.1 | convolution fusion | flops 268435456 | bytes 6553600 | tf_op jit(solution)/shard_map/while/body/eval_jaxpr/qhd,khd->qhk/dot_general | solution.py:59
  80.5 5.0 %fusion.133 = (f32[128,8]{0,1:T(8,128)S(1)}, f32[128,8,1024]{0,2,1:T(8,128)}) fusion(bf16[128,8,192]{0,2,1:T(8,128)(2,1)S(1)} %copy.109, bf16[1024,32]{0,1:T(8,128)(2,1)} %get-tuple-element.236, bf16[1024,32]{0,1:T(8,128)(2,1)} %get-tuple-element.237, f32[8,1024,128]{2,1,0:T(8,128)} %fusion.132), kind=kOutput, calls=%fused_computation.121.clone.1 | convolution fusion | flops 136576000 | bytes 8654848 | tf_op jit(solution)/shard_map/while/body/eval_jaxpr/qhr,kr->qhk/dot_general | solution.py:65
  85.5 2.9 %fusion.134 = f32[128,8]{0,1:T(8,128)S(1)} fusion(f32[128,8,1024]{0,2,1:T(8,128)} %get-tuple-element.240, f32[128,8]{0,1:T(8,128)S(1)} %select_maximum_fusion.2), kind=kLoop, calls=%fused_computation.4.clone.1 | loop fusion | flops 2096128 | bytes 4202496 | tf_op jit(solution)/shard_map/while/body/eval_jaxpr/reduce_sum | solution.py:74
  89.0 1.3 fusion.136
  93.6 2.7 %convolution_convert_fusion.5 = bf16[1024,2048]{1,0:T(8,128)(2,1)S(1)} fusion(bf16[256,2048]{1,0:T(8,128)(2,1)} %get-tuple-element.279, f32[256]{0:T(256)S(1)} %get-tuple-element.278, f32[1024]{0:T(1024)S(1)} %add_rsqrt_fusion.4, bf16[2048,256]{1,0:T(8,128)(2,1)} %get-tuple-element.277, s32[]{:T(128)S(6)} %select_n.22), kind=kOutput, calls=%fused_computation.2.clone.1 | convolution fusion | flops 1076887552 | bytes 5772292 | tf_op jit(solution)/shard_map/while/body/eval_jaxpr/dot_general | solution.py:48
  96.3 1.5 copy.110
  98.1 2.7 %fusion.132 = f32[8,1024,128]{2,1,0:T(8,128)} fusion(bf16[1024,8,128]{2,1,0:T(8,128)(2,1)S(1)} %get-tuple-element.238, bf16[128,8,192]{2,0,1:T(8,128)(2,1)S(1)} %get-tuple-element.280), kind=kOutput, calls=%fused_computation.7.clone.1 | convolution fusion | flops 268435456 | bytes 6553600 | tf_op jit(solution)/shard_map/while/body/eval_jaxpr/qhd,khd->qhk/dot_general | solution.py:59
  103.2 5.0 %fusion.133 = (f32[128,8]{0,1:T(8,128)S(1)}, f32[128,8,1024]{0,2,1:T(8,128)}) fusion(bf16[128,8,192]{0,2,1:T(8,128)(2,1)S(1)} %copy.109, bf16[1024,32]{0,1:T(8,128)(2,1)} %get-tuple-element.236, bf16[1024,32]{0,1:T(8,128)(2,1)} %get-tuple-element.237, f32[8,1024,128]{2,1,0:T(8,128)} %fusion.132), kind=kOutput, calls=%fused_computation.121.clone.1 | convolution fusion | flops 136576000 | bytes 8654848 | tf_op jit(solution)/shard_map/while/body/eval_jaxpr/qhr,kr->qhk/dot_general | solution.py:65
  108.2 2.9 %fusion.134 = f32[128,8]{0,1:T(8,128)S(1)} fusion(f32[128,8,1024]{0,2,1:T(8,128)} %get-tuple-element.240, f32[128,8]{0,1:T(8,128)S(1)} %select_maximum_fusion.2), kind=kLoop, calls=%fused_computation.4.clone.1 | loop fusion | flops 2096128 | bytes 4202496 | tf_op jit(solution)/shard_map/while/body/eval_jaxpr/reduce_sum | solution.py:74
  111.6 1.3 fusion.136
  115.2 3.9 %all_to_all.29 = bf16[2,64,1024]{2,1,0:T(8,128)(2,1)S(1)} all-to-all(bf16[2,64,1024]{2,1,0:T(8,128)(2,1)S(1)} %all_to_all.20), channel_id=1, replica_groups=mesh['sp'=16,'tp'=2] {'tp'}, dimensions={0} | all-to-all | bytes 524288 | tf_op jit(solution)/shard_map/all_to_all | solution.py:175
  119.2 5.1 %multiply_reduce_fusion = (f32[64]{0:T(128)S(1)}, f32[64,2048]{1,0:T(8,128)S(1)}) fusion(bf16[64,2048]{1,0:T(8,128)(2,1)S(1)} %bitcast.138, bf16[2048,2048]{1,0:T(8,128)(2,1)} %param.28, bf16[64,2048]{1,0:T(8,128)(2,1)S(1)} %copy-done.8), kind=kOutput, calls=%fused_computation.75 | convolution fusion | flops 537657280 | bytes 9437440 | tf_op jit(solution)/shard_map/dot_general | solution.py:176
  124.5 2.1 convolution_convert_fusion.3
  126.6 4.5 %all-to-all-start.1 = ((bf16[16,1,32,2048]{3,2,1,0:T(8,128)(2,1)}), bf16[16,1,32,2048]{3,2,1,0:T(8,128)(2,1)S(1)}, u32[]{:S(2)}, u32[]{:S(2)}) async-start(bf16[16,1,32,2048]{3,2,1,0:T(8,128)(2,1)} %bitcast.4), calls=%async_computation.1 | async-start | bytes 4194304 | tf_op jit(solution)/shard_map/all_to_all | solution.py:203
  132.5 41.9 %all-to-all-done.1 = bf16[16,1,32,2048]{3,2,1,0:T(8,128)(2,1)S(1)} async-done(((bf16[16,1,32,2048]{3,2,1,0:T(8,128)(2,1)}), bf16[16,1,32,2048]{3,2,1,0:T(8,128)(2,1)S(1)}, u32[]{:S(2)}, u32[]{:S(2)}) %all-to-all-start.1) | async-done | bytes 2097184 | tf_op jit(solution)/shard_map/all_to_all | solution.py:203
  174.4 3.8 %fusion.51 = f32[16,1,32,512]{3,2,0,1:T(8,128)} fusion(bf16[1,2048,512]{2,1,0:T(8,128)(2,1)} %all-gather.7.cloned.1.call-done, bf16[16,1,32,2048]{3,2,1,0:T(8,128)(2,1)S(1)} %all-to-all-done.1), kind=kOutput, calls=%fused_computation.65 | convolution fusion | flops 1073741824 | bytes 5242880 | tf_op jit(solution)/shard_map/secd,edf->secf/dot_general | solution.py:204
  178.2 3.2 %fusion.66 = bf16[16,1,32,512]{3,2,0,1:T(8,128)(2,1)S(1)} fusion(bf16[1,2048,512]{2,1,0:T(8,128)(2,1)} %all-gather.9.cloned.1.call-done, bf16[16,1,32,2048]{3,2,1,0:T(8,128)(2,1)S(1)} %all-to-all-done.1, f32[16,1,32,512]{3,2,0,1:T(8,128)} %fusion.51), kind=kOutput, calls=%fused_computation.68 | convolution fusion | flops 1075314688 | bytes 5767168 | tf_op jit(solution)/shard_map/secd,edf->secf/dot_general | solution.py:205
  181.5 2.1 convolution_convert_fusion.1
  183.6 2.0 fusion.40
  185.6 10.3 %all-to-all-start.2 = ((bf16[16,1,32,2048]{3,2,1,0:T(8,128)(2,1)}), bf16[16,1,32,2048]{3,2,1,0:T(8,128)(2,1)}, u32[]{:S(2)}, u32[]{:S(2)}) async-start(bf16[16,1,32,2048]{3,2,1,0:T(8,128)(2,1)} %fusion.40), calls=%async_computation.2 | async-start | bytes 4194304 | tf_op jit(solution)/shard_map/all_to_all | solution.py:221
  197.3 41.4 %all-to-all-done.2 = bf16[16,1,32,2048]{3,2,1,0:T(8,128)(2,1)} async-done(((bf16[16,1,32,2048]{3,2,1,0:T(8,128)(2,1)}), bf16[16,1,32,2048]{3,2,1,0:T(8,128)(2,1)}, u32[]{:S(2)}, u32[]{:S(2)}) %all-to-all-start.2) | async-done | bytes 2097184 | tf_op jit(solution)/shard_map/all_to_all | solution.py:221
  238.6 3.1 %convolution_add_fusion.1 = f32[64,2048]{1,0:T(8,128)} fusion(f32[64,2048]{1,0:T(8,128)} %copy-done.5, bf16[64,512]{1,0:T(8,128)(2,1)} %fusion.77, bf16[512,2048]{1,0:T(8,128)(2,1)} %bitcast.28), kind=kOutput, calls=%fused_computation.53 | convolution fusion | flops 134348800 | bytes 3211264 | tf_op jit(solution)/shard_map/dot_general | solution.py:222
  241.8 3.9 %fusion.43 = bf16[64,2048]{1,0:T(8,128)(2,1)} fusion(f32[64,2048]{1,0:T(8,128)} %convolution_add_fusion.1, bf16[512,2048]{1,0:T(8,128)(2,1)} %param.37, bf16[64,2048]{1,0:T(8,128)(2,1)S(1)} %multiply_convert_fusion, bf16[2048,512]{1,0:T(8,128)(2,1)} %param.36, f32[64,512]{1,0:T(8,128)S(1)} %fusion.96), kind=kOutput, calls=%fused_computation.57 | convolution fusion | flops 268894208 | bytes 5373952 | tf_op jit(solution)/shard_map/dot_general | solution.py:231
  (118 shorter events, 20.5 us)
Async XLA Ops:
  6.5 3.5 %copy-start = (bf16[512,3072]{1,0:T(8,128)(2,1)S(1)}, bf16[512,3072]{1,0:T(8,128)(2,1)}, u32[]{:S(2)}) copy-start(bf16[512,3072]{1,0:T(8,128)(2,1)} %param.26) | copy-start | bytes 9437188
  6.5 61.9 %all-gather.5.cloned.1.call-start = ((), (), s32[]{:S(2)}) async-start(), calls=%async_computation.3 | async-start | bytes 1114112 | tf_op jit(solution)/shard_map/all_gather | solution.py:90
  7.3 125.2 %all-gather.7.cloned.1.call-start = ((), (), s32[]{:S(2)}) async-start(), calls=%async_computation.4 | async-start | bytes 3145728 | tf_op jit(solution)/shard_map/all_gather | solution.py:129
  12.3 2.0 copy-start.13
  12.3 49.8 %copy-start.15 = (s32[64,4]{0,1:T(4,128)S(1)}, s32[64,4]{0,1:T(4,128)}, u32[]{:S(2)}) copy-start(s32[64,4]{0,1:T(4,128)} %param.30) | copy-start | bytes 3076
  14.0 54.4 %copy-start.10 = (f32[256]{0:T(256)S(1)}, f32[256]{0:T(256)}, u32[]{:S(2)}) copy-start(f32[256]{0:T(256)} %param.25) | copy-start | bytes 3076
  62.2 6.3 %copy-start.11 = (s32[64,4]{0,1:T(4,128)}, s32[64,4]{0,1:T(4,128)S(1)}, u32[]{:S(2)}) copy-start(s32[64,4]{0,1:T(4,128)S(1)} %multiply_add_fusion) | copy-start | bytes 3076
  68.4 5.2 %copy-start.17 = (s32[2]{0:T(128)}, s32[2]{0:T(128)S(1)}, u32[]{:S(2)}) copy-start(s32[2]{0:T(128)S(1)} %get-tuple-element.276) | copy-start | bytes 28 | tf_op jit(solution)/shard_map/while
  80.5 7.9 %copy-start.3 = (f32[128,8,128]{0,2,1:T(8,128)S(1)}, f32[128,8,128]{0,2,1:T(8,128)}, u32[]{:S(2)}) copy-start(f32[128,8,128]{0,2,1:T(8,128)} %get-tuple-element.261) | copy-start | bytes 1572868 | tf_op jit(solution)/shard_map/while
  85.5 3.4 %copy-start.2 = (f32[128,8,1024]{0,2,1:T(8,128)S(1)}, f32[128,8,1024]{0,2,1:T(8,128)}, u32[]{:S(2)}) copy-start(f32[128,8,1024]{0,2,1:T(8,128)} %get-tuple-element.240) | copy-start | bytes 12582916 | tf_op jit(solution)/shard_map/while
  89.0 2.1 copy-start.18
  90.3 0.8 copy-start.4
  91.1 5.2 %copy-start.17 = (s32[2]{0:T(128)}, s32[2]{0:T(128)S(1)}, u32[]{:S(2)}) copy-start(s32[2]{0:T(128)S(1)} %get-tuple-element.276) | copy-start | bytes 28 | tf_op jit(solution)/shard_map/while
  103.2 7.9 %copy-start.3 = (f32[128,8,128]{0,2,1:T(8,128)S(1)}, f32[128,8,128]{0,2,1:T(8,128)}, u32[]{:S(2)}) copy-start(f32[128,8,128]{0,2,1:T(8,128)} %get-tuple-element.261) | copy-start | bytes 1572868 | tf_op jit(solution)/shard_map/while
  108.2 3.4 %copy-start.2 = (f32[128,8,1024]{0,2,1:T(8,128)S(1)}, f32[128,8,1024]{0,2,1:T(8,128)}, u32[]{:S(2)}) copy-start(f32[128,8,1024]{0,2,1:T(8,128)} %get-tuple-element.240) | copy-start | bytes 12582916 | tf_op jit(solution)/shard_map/while
  111.6 2.1 copy-start.18
  112.9 0.8 copy-start.4
  113.8 5.4 %copy-start.8 = (bf16[64,2048]{1,0:T(8,128)(2,1)S(1)}, bf16[64,2048]{1,0:T(8,128)(2,1)}, u32[]{:S(2)}) copy-start(bf16[64,2048]{1,0:T(8,128)(2,1)} %param.20) | copy-start | bytes 786436
  119.2 5.1 %copy-start.14 = (f32[2048]{0:T(1024)S(1)}, f32[2048]{0:T(1024)}, u32[]{:S(2)}) copy-start(f32[2048]{0:T(1024)} %param.29) | copy-start | bytes 24580
  119.2 5.2 %copy-start.9 = (pred[64,512]{1,0:T(8,128)(4,1)S(1)}, pred[64,512]{1,0:T(8,128)(4,1)}, u32[]{:S(2)}) copy-start(pred[64,512]{1,0:T(8,128)(4,1)} %fusion.72) | copy-start | bytes 98308
  124.3 2.3 copy-start.5
  126.6 47.8 %all-to-all-start.1 = ((bf16[16,1,32,2048]{3,2,1,0:T(8,128)(2,1)}), bf16[16,1,32,2048]{3,2,1,0:T(8,128)(2,1)S(1)}, u32[]{:S(2)}, u32[]{:S(2)}) async-start(bf16[16,1,32,2048]{3,2,1,0:T(8,128)(2,1)} %bitcast.4), calls=%async_computation.1 | async-start | bytes 4194304 | tf_op jit(solution)/shard_map/all_to_all | solution.py:203
  131.1 47.1 %all-gather.9.cloned.1.call-start = ((), (), s32[]{:S(2)}) async-start(), calls=%async_computation.5 | async-start | bytes 3145728 | tf_op jit(solution)/shard_map/all_gather | solution.py:130
  131.9 49.6 %all-gather.11.cloned.1.call-start = ((), (), s32[]{:S(2)}) async-start(), calls=%async_computation.6 | async-start | bytes 3145728 | tf_op jit(solution)/shard_map/all_gather | solution.py:131
  181.5 2.1 copy-start.7
  185.6 10.4 %copy-start.16 = (f32[64,4]{0,1:T(4,128)S(1)}, f32[64,4]{0,1:T(4,128)}, u32[]{:S(2)}) copy-start(f32[64,4]{0,1:T(4,128)} %param.31) | copy-start | bytes 3076
  185.6 10.4 %copy-start.12 = (s32[64,4]{0,1:T(4,128)S(1)}, s32[64,4]{0,1:T(4,128)}, u32[]{:S(2)}) copy-start(s32[64,4]{0,1:T(4,128)} %copy-done.11) | copy-start | bytes 3076
  185.6 11.2 %copy-start.6 = (bf16[2048,512]{1,0:T(8,128)(2,1)S(1)}, bf16[2048,512]{1,0:T(8,128)(2,1)}, u32[]{:S(2)}) copy-start(bf16[2048,512]{1,0:T(8,128)(2,1)} %param.35) | copy-start | bytes 6291460
  185.6 53.0 %all-to-all-start.2 = ((bf16[16,1,32,2048]{3,2,1,0:T(8,128)(2,1)}), bf16[16,1,32,2048]{3,2,1,0:T(8,128)(2,1)}, u32[]{:S(2)}, u32[]{:S(2)}) async-start(bf16[16,1,32,2048]{3,2,1,0:T(8,128)(2,1)} %fusion.40), calls=%async_computation.2 | async-start | bytes 4194304 | tf_op jit(solution)/shard_map/all_to_all | solution.py:221
  238.6 7.1 %copy-start.1 = (bf16[512,3072]{1,0:T(8,128)(2,1)S(1)}, bf16[512,3072]{1,0:T(8,128)(2,1)}, u32[]{:S(2)}) copy-start(bf16[512,3072]{1,0:T(8,128)(2,1)} %param.26) | copy-start | bytes 9437188
Sparse Core Ops, SparseCore 0:
  10.1 58.2 all-gather.4
  69.9 8.9 all-gather.6
  133.5 11.3 all-gather.8
  146.3 11.7 all-gather.10
where the time goes:
time: 257 us; the launch traced here: 252 us
  waiting for transfers between devices  89.1 us (35%)
  matrix products  51.4 us (20%)
  blocking collectives  50.7 us (20%)
  other arithmetic  17.4 us (7%)
  starting transfers between devices  15 us (6%)
  local copies, waits for them, and re-layouts  13.6 us (5%)
  between operations  13.5 us (5%)
    all_gather x1, blocking collectives, attend_all(): rot_piece = lax.all_gather(rot_shard, 'sp', axis=0, tiled=True)  46.8 us
    all_to_all x1, waiting for transfers between devices, shards(): lax.all_to_all(outgoing, 'sp', split_axis=0, concat_axis=0, tiled=True)  41.9 us
    all_to_all x1, waiting for transfers between devices, shards(): lax.all_to_all(summed, 'sp', split_axis=0, concat_axis=0, tiled=True)  41.4 us
    all_to_all x1, starting transfers between devices, shards(): lax.all_to_all(summed, 'sp', split_axis=0, concat_axis=0, tiled=True)  10.3 us
    dot_general x2, matrix products, absorb(): jnp.einsum('qhr,kr->qhk', queries[:, :, KEY_PLAIN_WIDTH:], shared_rot, pr...  10 us
    while x26, local copies, waits for them, and re-layouts  6.17 us
    reduce_sum x2, other arithmetic, absorb(): new_sum = run_sum * factor + jnp.sum(weights, axis=-1)  5.81 us
    dot_general x2, matrix products, expand_keys(): jnp.dot(keyval_normed, keyval_cols, preferred_element_type=jnp.float32)  5.38 us
  transfers between devices with their start and end apart: 6, of which 3 were waited for; matrix products, arithmetic and copies ran while one was open for 27% of the time, Pallas kernels for 0%

commit v1 on v0

v1 whole, which is shorter than its diff:
```python
import functools

import jax
import jax.numpy as jnp
from jax import lax
from jax.experimental import pallas as pl
from jax.experimental.pallas import tpu as pltpu
from jax.sharding import PartitionSpec as P

KEY_PLAIN_WIDTH = 128
ROTARY_WIDTH = 64
VALUE_HEAD_WIDTH = 128
LANES = 128

epsilon = 1e-06
routed_scale = 2.5
theta_base = 10000.0
MESH = pl.DeviceIdType.MESH
F32 = jnp.float32
BF16 = jnp.bfloat16


def rms_scale(values, scales):
    widened = values.astype(F32)
    inverse = lax.rsqrt(jnp.mean(widened * widened, axis=-1, keepdims=True) + epsilon)
    return widened * inverse * scales


def turn_tables(positions, rot_width):
    half_width = rot_width // 2
    frequency = theta_base ** (-(jnp.arange(half_width, dtype=F32) * 2.0) / rot_width)
    angles = positions.astype(F32)[:, None] * frequency[None, :]
    return (jnp.cos(angles), jnp.sin(angles))


def turn(values, cos_part, sine_part):
    lower_half, upper_half = jnp.split(values, 2, axis=-1)
    return jnp.concatenate(
        [
            lower_half * cos_part - upper_half * sine_part,
            upper_half * cos_part + lower_half * sine_part,
        ],
        axis=-1,
    )


def line_length(n):
    for candidate in (4, 2):
        if n % candidate == 0:
            return candidate
    return 1


def remote(src, dst, send_sem, recv_sem, sp, tp):
    return pltpu.make_async_remote_copy(
        src_ref=src,
        dst_ref=dst,
        send_sem=send_sem,
        recv_sem=recv_sem,
        device_id=(sp, tp),
        device_id_type=MESH,
    )


def greet(n, nz, with_partner):
    pn = n // nz
    me, t = lax.axis_index("sp"), lax.axis_index("tp")
    z, p = me // pn, me % pn
    barrier = pltpu.get_barrier_semaphore()
    for dz in range(1, nz):
        pl.semaphore_signal(
            barrier, inc=1, device_id=(((z + dz) % nz) * pn + p, t), device_id_type=MESH
        )
    for d in range(1, pn):
        pl.semaphore_signal(
            barrier, inc=1, device_id=(z * pn + (p + d) % pn, t), device_id_type=MESH
        )
    if with_partner:
        pl.semaphore_signal(barrier, inc=1, device_id=(me, 1 - t), device_id_type=MESH)
    pl.semaphore_wait(barrier, nz - 1 + pn - 1 + (1 if with_partner else 0))


def gather_kernel(
    n, nz, x_ref, g_ref, u_ref, d_ref, kv_ref, go_ref, uo_ref, do_ref,
    zs, zr, ps, pr, xs, xr, ws, wr,
):
    pn = n // nz
    me, t = lax.axis_index("sp"), lax.axis_index("tp")
    z, p = me // pn, me % pn
    greet(n, nz, True)

    def block_of(dz, d):
        return ((z - dz + nz) % nz) * pn + (p - d + pn) % pn

    def along(dz):
        return remote(
            x_ref.at[t], kv_ref.at[me, t], zs.at[dz], zr.at[dz], ((z + dz) % nz) * pn + p, t
        )

    def across(dz, d):
        b = block_of(dz, 0)
        src = x_ref.at[t] if dz == 0 else kv_ref.at[b, t]
        return remote(
            src, kv_ref.at[b, t], ps.at[dz, d], pr.at[dz, d], z * pn + (p + d) % pn, t
        )

    def swap(dz, d):
        b = block_of(dz, d)
        return remote(
            kv_ref.at[b, t], kv_ref.at[b, t], xs.at[dz, d], xr.at[dz, d], me, 1 - t
        )

    weights = [
        remote(g_ref, go_ref, ws.at[0], wr.at[0], me, 1 - t),
        remote(u_ref, uo_ref, ws.at[1], wr.at[1], me, 1 - t),
        remote(d_ref, do_ref, ws.at[2], wr.at[2], me, 1 - t),
    ]
    for dz in range(1, nz):
        along(dz).start()
    for d in range(1, pn):
        across(0, d).start()
    for copy in weights:
        copy.start()
    kv_ref[me] = x_ref[...]
    for dz in range(1, nz):
        along(dz).wait_recv()
        for d in range(1, pn):
            across(dz, d).start()
        swap(dz, 0).start()
    for dz in range(nz):
        for d in range(1, pn):
            across(dz, d).wait_recv()
            swap(dz, d).start()
    for dz in range(nz):
        for d in range(pn):
            if dz or d:
                swap(dz, d).wait()
    for dz in range(1, nz):
        along(dz).wait_send()
    for dz in range(nz):
        for d in range(1, pn):
            across(dz, d).wait_send()
    for copy in weights:
        copy.wait()


def gather_latents(n, nz, packed, gate, up, down):
    pn = n // nz
    rows, width = packed.shape
    anywhere = pl.BlockSpec(memory_space=pl.ANY)
    inside = pl.BlockSpec(memory_space=pltpu.VMEM)
    return pl.pallas_call(
        functools.partial(gather_kernel, n, nz),
        out_shape=(
            jax.ShapeDtypeStruct((n, 2, rows // 2, width), BF16),
            jax.ShapeDtypeStruct(gate.shape, BF16),
            jax.ShapeDtypeStruct(up.shape, BF16),
            jax.ShapeDtypeStruct(down.shape, BF16),
        ),
        in_specs=[inside, anywhere, anywhere, anywhere],
        out_specs=(inside, anywhere, anywhere, anywhere),
        scratch_shapes=[
            pltpu.SemaphoreType.DMA((nz,)),
            pltpu.SemaphoreType.DMA((nz,)),
            pltpu.SemaphoreType.DMA((nz, pn)),
            pltpu.SemaphoreType.DMA((nz, pn)),
            pltpu.SemaphoreType.DMA((nz, pn)),
            pltpu.SemaphoreType.DMA((nz, pn)),
            pltpu.SemaphoreType.DMA((3,)),
            pltpu.SemaphoreType.DMA((3,)),
        ],
        compiler_params=pltpu.CompilerParams(collective_id=0, has_side_effects=True),
        name="gather_latents",
    )(packed.reshape(2, rows // 2, width), gate, up, down)


NT = (((1,), (1,)), ((), ()))
TN = (((0,), (0,)), ((), ()))


def attend_kernel(heads, t_ref, qn_ref, qr_ref, w_ref, kv_ref, out_ref):
    latent = kv_ref.shape[1] - LANES
    pair = KEY_PLAIN_WIDTH + VALUE_HEAD_WIDTH
    rows = qn_ref.shape[1]
    parts = []
    for h in range(heads):
        wk = w_ref[:, h * pair : h * pair + KEY_PLAIN_WIDTH]
        qa = lax.dot_general(qn_ref[h], wk, NT, preferred_element_type=F32).astype(BF16)
        parts.append(jnp.concatenate([qa, qr_ref[h]], axis=1))
    q = jnp.concatenate(parts, axis=0)
    scores = lax.dot_general(q, kv_ref[...], NT, preferred_element_type=F32)
    weights = jnp.exp(scores - jnp.max(scores, axis=-1, keepdims=True))
    total = jnp.sum(weights, axis=-1, keepdims=True)
    mixed = jnp.dot(weights.astype(BF16), kv_ref[:, :latent], preferred_element_type=F32)
    mixed = (mixed / total).astype(BF16)
    for h in range(heads):
        wv = w_ref[:, h * pair + KEY_PLAIN_WIDTH : (h + 1) * pair]
        out_ref[:, h * VALUE_HEAD_WIDTH : (h + 1) * VALUE_HEAD_WIDTH] = jnp.dot(
            mixed[h * rows : (h + 1) * rows], wv, preferred_element_type=F32
        ).astype(BF16)


def attend(tp_index, plain, rotary, weight, kv, heads):
    local_heads, rows, _ = plain.shape
    steps = local_heads // heads
    pair = KEY_PLAIN_WIDTH + VALUE_HEAD_WIDTH
    return pl.pallas_call(
        functools.partial(attend_kernel, heads),
        grid_spec=pltpu.PrefetchScalarGridSpec(
            num_scalar_prefetch=1,
            grid=(steps,),
            in_specs=[
                pl.BlockSpec((heads, rows, LANES), lambda i, t: (i, 0, 0)),
                pl.BlockSpec((heads, rows, LANES), lambda i, t: (i, 0, 0)),
                pl.BlockSpec((weight.shape[0], heads * pair), lambda i, t: (0, t[0] * steps + i)),
                pl.BlockSpec(kv.shape, lambda i, t: (0, 0)),
            ],
            out_specs=pl.BlockSpec((rows, heads * VALUE_HEAD_WIDTH), lambda i, t: (0, i)),
        ),
        out_shape=jax.ShapeDtypeStruct((rows, local_heads * VALUE_HEAD_WIDTH), BF16),
        compiler_params=pltpu.CompilerParams(vmem_limit_bytes=60 * 1024 * 1024),
        name="attend",
    )(tp_index.reshape(1), plain, rotary, weight, kv)


def silu(v):
    return v / (1.0 + jnp.exp(-v))


def moe_kernel(
    n, nz, cap,
    normed_ref, stream_ref, maps_ref, g_ref, u_ref, d_ref, go_ref, uo_ref, do_ref,
    sg_ref, su_ref, sd_ref, out_ref,
    wg, wu, wd, sg, su, sd, zb, zm, sb, ab, ob, rb, pb, qb, acc,
    ls, zs, zr, ms, mr, ps, pr, rs, rr, cs, cr,
):
    pn = n // nz
    slots = pn * cap
    width = normed_ref.shape[1]
    me, t = lax.axis_index("sp"), lax.axis_index("tp")
    z, p = me // pn, me % pn
    loads = [
        pltpu.make_async_copy(src, dst, ls.at[i])
        for i, (src, dst) in enumerate(
            [
                (g_ref, wg.at[0]), (go_ref, wg.at[1]), (u_ref, wu.at[0]), (uo_ref, wu.at[1]),
                (d_ref, wd.at[0]), (do_ref, wd.at[1]), (sg_ref, sg), (su_ref, su), (sd_ref, sd),
            ]
        )
    ]
    for copy in loads:
        copy.start()
    greet(n, nz, False)

    def ahead(dz):
        return ((z + dz) % nz) * pn + p

    def rows_along(dz):
        return remote(normed_ref, zb.at[dz], zs.at[dz], zr.at[dz], ahead(dz), t)

    def maps_along(dz):
        return remote(
            maps_ref.at[(z + dz) % nz], zm.at[dz], ms.at[dz], mr.at[dz], ahead(dz), t
        )

    def across(dz, d):
        q = (p + d) % pn
        return remote(
            sb.at[dz, q], ab.at[dz, d], ps.at[dz, d], pr.at[dz, d], z * pn + q, t
        )

    def back(dz, d):
        q = (p - d + pn) % pn
        return remote(
            ob.at[dz, d], rb.at[dz, p], rs.at[dz, d], rr.at[dz, d], z * pn + q, t
        )

    def home(dz):
        return remote(
            pb.at[dz], qb.at[dz], cs.at[dz], cr.at[dz], ((z - dz + nz) % nz) * pn + p, t
        )

    for dz in range(1, nz):
        maps_along(dz).start()
        rows_along(dz).start()
    zb[0] = normed_ref[...]
    zm[0] = maps_ref[z]

    def pick(dz, carried):
        @pl.when(dz > 0)
        def _():
            maps_along(dz).wait_recv()
            rows_along(dz).wait_recv()

        chosen = lax.dot_general(
            zm[dz][:, :slots], zb[dz], TN, preferred_element_type=F32
        )
        for q in range(pn):
            sb[dz, q] = chosen[q * cap : (q + 1) * cap].astype(BF16)
        ab[dz, 0] = sb[dz, p]
        for d in range(1, pn):
            across(dz, d).start()
        return carried

    lax.fori_loop(0, nz, pick, 0)
    for copy in loads:
        copy.wait()
    normed = normed_ref[...]
    shared_inner = (
        silu(jnp.dot(normed, sg[...], preferred_element_type=F32))
        * jnp.dot(normed, su[...], preferred_element_type=F32)
    ).astype(BF16)
    acc[...] = stream_ref[...].astype(F32) + jnp.dot(
        shared_inner, sd[...], preferred_element_type=F32
    )

    def stack(ref, dz):
        if cap % 16 == 0:
            return ref[dz].reshape(slots, width)
        return jnp.concatenate([ref[dz, d].astype(F32) for d in range(pn)], axis=0).astype(BF16)

    def expert(dz, carried):
        for d in range(1, pn):
            across(dz, d).wait_recv()
        rows = stack(ab, dz)
        halves = []
        for h in range(2):
            gate_act = jnp.dot(rows, wg[h], preferred_element_type=F32)
            up_act = jnp.dot(rows, wu[h], preferred_element_type=F32)
            inner = (silu(gate_act) * up_act).astype(BF16)
            halves.append(jnp.dot(inner, wd[h], preferred_element_type=F32).astype(BF16))
        summed = halves[0].astype(F32) + halves[1].astype(F32)
        for d in range(pn):
            ob[dz, d] = summed[d * cap : (d + 1) * cap].astype(BF16)
        rb[dz, p] = ob[dz, 0]
        for d in range(1, pn):
            back(dz, d).start()
        return carried

    lax.fori_loop(0, nz, expert, 0)

    def combine(dz, carried):
        for d in range(1, pn):
            back(dz, d).wait_recv()
        part = jnp.dot(zm[dz][:, slots:], stack(rb, dz), preferred_element_type=F32)

        @pl.when(dz == 0)
        def _():
            acc[...] += part

        @pl.when(dz > 0)
        def _():
            pb[dz] = part.astype(BF16)
            home(dz).start()

        return carried

    lax.fori_loop(0, nz, combine, 0)
    total = acc[...]
    for dz in range(1, nz):
        home(dz).wait_recv()
        total = total + qb[dz].astype(F32)
    out_ref[...] = total.astype(BF16)
    for dz in range(1, nz):
        maps_along(dz).wait_send()
        rows_along(dz).wait_send()
        home(dz).wait_send()
    for dz in range(nz):
        for d in range(1, pn):
            across(dz, d).wait_send()
            back(dz, d).wait_send()


def experts(n, nz, cap, normed, stream, maps, weights, shared):
    pn = n // nz
    rows, width = normed.shape
    hidden = weights[0].shape[1]
    shared_hidden = shared[0].shape[1]
    anywhere = pl.BlockSpec(memory_space=pl.ANY)
    inside = pl.BlockSpec(memory_space=pltpu.VMEM)
    plane = (nz, pn, cap, width)
    dma = pltpu.SemaphoreType.DMA
    return pl.pallas_call(
        functools.partial(moe_kernel, n, nz, cap),
        out_shape=jax.ShapeDtypeStruct((rows, width), BF16),
        in_specs=[inside] * 3 + [anywhere] * 9,
        out_specs=inside,
        scratch_shapes=[
            pltpu.VMEM((2, width, hidden), BF16),
            pltpu.VMEM((2, width, hidden), BF16),
            pltpu.VMEM((2, hidden, width), BF16),
            pltpu.VMEM((width, shared_hidden), BF16),
            pltpu.VMEM((width, shared_hidden), BF16),
            pltpu.VMEM((shared_hidden, width), BF16),
            pltpu.VMEM((nz, rows, width), BF16),
            pltpu.VMEM((nz, rows, maps.shape[2]), BF16),
            pltpu.VMEM(plane, BF16),
            pltpu.VMEM(plane, BF16),
            pltpu.VMEM(plane, BF16),
            pltpu.VMEM(plane, BF16),
            pltpu.VMEM((nz, rows, width), BF16),
            pltpu.VMEM((nz, rows, width), BF16),
            pltpu.VMEM((rows, width), F32),
            dma((9,)),
            dma((nz,)), dma((nz,)), dma((nz,)), dma((nz,)),
            dma((nz, pn)), dma((nz, pn)), dma((nz, pn)), dma((nz, pn)),
            dma((nz,)), dma((nz,)),
        ],
        compiler_params=pltpu.CompilerParams(
            collective_id=1, has_side_effects=True, vmem_limit_bytes=60 * 1024 * 1024
        ),
        name="experts",
    )(normed, stream, maps, *weights, *shared)


def shards(
    n,
    stream_in,
    query_compressed,
    keyvalue_compressed,
    rope_key,
    query_norm_gain,
    keyvalue_norm_gain,
    query_up_weight,
    keyvalue_up_weight,
    out_proj,
    ffn_gain,
    expert_ids,
    expert_weights,
    expert_gate,
    expert_up,
    expert_down,
    shared_gate,
    shared_up,
    shared_down,
):
    nz = line_length(n)
    tok_rows = query_compressed.shape[0]
    head_width = KEY_PLAIN_WIDTH + ROTARY_WIDTH
    all_heads = query_up_weight.shape[1] // head_width
    local_heads = all_heads // 2
    sp_index = lax.axis_index("sp")
    tp_index = lax.axis_index("tp")
    own_pos = sp_index * tok_rows + jnp.arange(tok_rows, dtype=jnp.int32)
    cos_part, sine_part = turn_tables(own_pos, ROTARY_WIDTH)

    keyval_normed = rms_scale(keyvalue_compressed, keyvalue_norm_gain).astype(BF16)
    shared_rot = turn(rope_key.astype(F32), cos_part, sine_part).astype(BF16)
    fill = jnp.zeros((tok_rows, LANES - ROTARY_WIDTH), BF16)
    packed = jnp.concatenate([keyval_normed, shared_rot, fill], axis=1)
    kv, gate_other, up_other, down_other = gather_latents(
        n, nz, packed, expert_gate[0], expert_up[0], expert_down[0]
    )
    kv = kv.reshape(n * tok_rows, packed.shape[1])

    query_normed = rms_scale(query_compressed, query_norm_gain).astype(BF16)
    query_cols = lax.dynamic_slice_in_dim(
        query_up_weight, tp_index * local_heads * head_width, local_heads * head_width, 1
    )
    raw_query = jnp.dot(query_normed, query_cols, preferred_element_type=F32) * head_width ** (-0.5)
    raw_query = raw_query.reshape(tok_rows, local_heads, head_width)
    turned = turn(raw_query[:, :, KEY_PLAIN_WIDTH:], cos_part[:, None, :], sine_part[:, None, :])
    plain = jnp.transpose(raw_query[:, :, :KEY_PLAIN_WIDTH].astype(BF16), (1, 0, 2))
    rotary = jnp.transpose(
        jnp.pad(turned.astype(BF16), ((0, 0), (0, 0), (0, LANES - ROTARY_WIDTH))), (1, 0, 2)
    )
    local_out = attend(tp_index, plain, rotary, keyvalue_up_weight, kv, 2)

    attended = lax.all_to_all(local_out, "tp", split_axis=0, concat_axis=1, tiled=True)
    projected = jnp.dot(attended, out_proj, preferred_element_type=F32)
    stream = (stream_in.astype(F32) + projected).astype(BF16)
    normed = rms_scale(stream, ffn_gain).astype(BF16)

    shares = (
        routed_scale * expert_weights / jnp.sum(expert_weights, axis=-1, keepdims=True)
    ).astype(BF16)
    moe_rows = stream_in.shape[0]
    top_count = expert_ids.shape[1]
    expert_count = expert_gate.shape[0] * n
    capacity = 2 * moe_rows * top_count // expert_count
    slots = expert_count // nz * capacity
    flat_ids = expert_ids.reshape(-1)
    hot_ids = (flat_ids[:, None] == jnp.arange(expert_count, dtype=jnp.int32)[None, :]).astype(
        jnp.int32
    )
    rank_ids = jnp.sum((jnp.cumsum(hot_ids, axis=0) - hot_ids) * hot_ids, axis=1)
    slot_ids = flat_ids * capacity + rank_ids
    hot_slots = (
        slot_ids[:, None] == jnp.arange(expert_count * capacity, dtype=jnp.int32)[None, :]
    ).reshape(moe_rows, top_count, expert_count * capacity)
    sender_map = jnp.any(hot_slots, axis=1).astype(BF16).reshape(moe_rows, nz, slots)
    share_map = jnp.sum(
        jnp.where(hot_slots, shares[:, :, None], jnp.zeros((), BF16)), axis=1
    ).reshape(moe_rows, nz, slots)
    maps = jnp.transpose(jnp.concatenate([sender_map, share_map], axis=2), (1, 0, 2))
    return experts(
        n, nz, capacity, normed, stream, maps,
        (expert_gate[0], expert_up[0], expert_down[0], gate_other, up_other, down_other),
        (shared_gate, shared_up, shared_down),
    )


def solution(mesh):
    in_specs = (
        P(("sp", "tp"), None),
        P("sp", None),
        P("sp", None),
        P("sp", None),
        P(),
        P(),
        P(),
        P(),
        P(),
        P(),
        P(("sp", "tp"), None),
        P(("sp", "tp"), None),
        P("sp", None, "tp"),
        P("sp", None, "tp"),
        P("sp", "tp", None),
        P(),
        P(),
        P(),
    )
    return jax.shard_map(
        functools.partial(shards, mesh.shape["sp"]),
        mesh=mesh,
        in_specs=in_specs,
        out_specs=P(("sp", "tp"), None),
        check_vma=False,
    )
```

time: 257 us -> 142 us (0.55); the launches traced: 252 us -> 141 us
  Pallas kernels: 0 us -> 107 us
  waiting for transfers between devices: 89.1 us -> 1.22 us
  blocking collectives: 50.7 us -> 0 us
  matrix products: 51.4 us -> 7.34 us
  between operations: 13.5 us -> 0.22 us
  starting transfers between devices: 15 us -> 3.44 us
  other arithmetic: 17.4 us -> 9.86 us
    pallas_call x0 -> x3, Pallas kernels: none -> 107 us  [the longest x1 76.3 us: experts(): pl.pallas_call(functools.partial(moe_kernel, n, nz, cap), out_shape=jax.S...]
    all_to_all x2 -> x1, waiting for transfers between devices: 83.3 us -> 1.22 us  [shards(): lax.all_to_all(local_out, 'tp', split_axis=0, concat_axis=1, tiled=True)]
    all_gather x1 -> x0, blocking collectives: 46.8 us -> none  [attend_all(): rot_piece = lax.all_gather(rot_shard, 'sp', axis=0, tiled=True)]
    dot_general x18 -> x2, matrix products: 51.4 us -> 7.34 us  [the longest x1 5.1 us: shards(): projected = jnp.dot(attended, out_proj, preferred_element_type=F32)]
    all_to_all x2 -> x1, starting transfers between devices: 14.9 us -> 3.44 us  [shards(): lax.all_to_all(local_out, 'tp', split_axis=0, concat_axis=1, tiled=True)]
    reduce_sum x3 -> x1, other arithmetic: 6.58 us -> 0.14 us  [shards(): jnp.sum(jnp.where(hot_slots, shares[:, :, None], jnp.zeros((), BF16)), ax...]
    while x26 -> x0, local copies, waits for them, and re-layouts: 6.17 us -> none
    unnamed x30 -> x19, local copies, waits for them, and re-layouts: 1.05 us -> 6.37 us
  transfers between devices with their start and end apart: 6 -> 1, of which waited for: 3 -> 1; matrix products, arithmetic and copies ran while one was open for 27% -> 0% of each run, Pallas kernels for 0% -> 0%
where the time goes in v1:
time: 142 us; the launch traced here: 141 us
  Pallas kernels  107 us (75%)
  local copies, waits for them, and re-layouts  12.5 us (9%)
  other arithmetic  9.86 us (7%)
  matrix products  7.34 us (5%)
  starting transfers between devices  3.44 us (2%)
    pallas_call x1, Pallas kernels, experts(): pl.pallas_call(functools.partial(moe_kernel, n, nz, cap), out_shape=jax.S...  76.3 us
    pallas_call x1, Pallas kernels, gather_latents(): pl.pallas_call(functools.partial(gather_kernel, n, nz), out_shape=(jax.Sh...  20.1 us
    pallas_call x1, Pallas kernels, attend(): pl.pallas_call(functools.partial(attend_kernel, heads), grid_spec=pltpu.P...  10.4 us
    unnamed x19, local copies, waits for them, and re-layouts  6.37 us
    dot_general x1, matrix products, shards(): projected = jnp.dot(attended, out_proj, preferred_element_type=F32)  5.1 us
    all_to_all x1, starting transfers between devices, shards(): lax.all_to_all(local_out, 'tp', split_axis=0, concat_axis=1, tiled=True)  3.44 us
  transfers between devices with their start and end apart: 1, of which 1 were waited for; matrix products, arithmetic and copies ran while one was open for 0% of the time, Pallas kernels for 0%

profile of v1, /device:TPU:0, one launch (start us, length us, event | category | flops | bytes accessed | tf_op | source)
XLA Modules:
  0.0 141.3 jit_solution(811387364197543519)
XLA Ops:
  0.0 1.2 fusion.9
  1.2 0.8 copy-done
  2.0 2.2 %convolution_multiply_fusion = f32[128,1536]{1,0:T(8,128)} fusion(bf16[512,3072]{1,0:T(8,128)(2,1)S(1)} %copy-done, s32[]{:T(128)S(6)} %select_n.7, bf16[128,512]{1,0:T(8,128)(2,1)} %param.19, f32[512]{0:T(512)} %param.22, f32[128]{0:T(128)S(1)} %add_rsqrt_fusion.2), kind=kOutput, calls=%fused_computation | convolution fusion | flops 201785344 | bytes 2492932 | tf_op jit(solution)/shard_map/dot_general | solution.py:460
  4.2 2.3 %copy.76 = f32[128,1536]{0,1:T(8,128)} copy(f32[128,1536]{1,0:T(8,128)} %convolution_multiply_fusion) | data formatting | bytes 1572864 | tf_op jit(solution)/shard_map/mul | solution.py:460
  6.5 1.1 slice.20
  7.6 1.6 %fusion.27 = (f32[128,8,32]{0,2,1:T(8,128)}, f32[128,8,32]{0,2,1:T(8,128)S(1)}) fusion(f32[128,8,192]{0,2,1:T(8,128)} %bitcast.54), kind=kLoop, calls=%fused_computation.60 | loop fusion | bytes 524288 | tf_op jit(solution)/shard_map/split | solution.py:37
  9.2 0.6 multiply_power_fusion
  9.8 0.8 copy.91
  10.7 1.9 %copy.93 = f32[128,8,32]{2,0,1:T(8,128)} copy(f32[128,8,32]{0,2,1:T(8,128)} %get-tuple-element.15) | data formatting | bytes 262144
  12.6 1.0 copy.92
  13.6 0.8 subtract_convert_fusion.1
  14.7 0.1 copy.83
  14.8 0.1 copy.82
  14.9 1.0 fusion.15
  15.9 1.4 subtract_convert_fusion
  17.2 0.9 fusion.14.qr_ref
  18.1 0.8 fusion.17
  19.0 0.7 maximum_maximum_fusion
  19.7 20.1 %gather_latents.1 = (bf16[16,2,64,384]{3,2,1,0:T(8,128)(2,1)}, bf16[2048,256]{1,0:T(8,128)(2,1)}, bf16[2048,256]{1,0:T(8,128)(2,1)}, bf16[256,2048]{1,0:T(8,128)(2,1)}) custom-call(bf16[2,64,384]{2,1,0:T(8,128)(2,1)} %bitcast.60, bf16[2048,256]{1,0:T(8,128)(2,1)} %bitcast.47, bf16[2048,256]{1,0:T(8,128)(2,1)} %bitcast.49, bf16[256,2048]{1,0:T(8,128)(2,1)} %bitcast.51), custom_call_target="tpu_custom_call" | custom-call | tf_op jit(solution)/shard_map/gather_latents/pallas_call | solution.py:152
  39.8 10.4 %attend.1 = bf16[128,1024]{1,0:T(8,128)(2,1)} custom-call(s32[1]{0:T(128)} %bitcast.t_ref, bf16[8,128,128]{2,1,0:T(8,128)(2,1)} %bitcast.57, bf16[8,128,128]{2,1,0:T(8,128)(2,1)} %fusion.14.qr_ref, bf16[256,4096]{1,0:T(8,128)(2,1)} %w_ref.1, bf16[2048,384]{1,0:T(8,128)(2,1)} %bitcast.56), custom_call_target="tpu_custom_call" | custom-call | tf_op jit(solution)/shard_map/attend/pallas_call | solution.py:207
  50.2 3.4 %all-to-all-start = ((bf16[2,64,1024]{2,1,0:T(8,128)(2,1)}), bf16[2,64,1024]{2,1,0:T(8,128)(2,1)S(1)}, u32[]{:S(2)}, u32[]{:S(2)}) async-start(bf16[2,64,1024]{2,1,0:T(8,128)(2,1)} %bitcast.58), calls=%async_computation | async-start | bytes 524288 | tf_op jit(solution)/shard_map/all_to_all | solution.py:469
  53.9 1.2 all-to-all-done
  55.2 5.1 %fusion.2 = (f32[64]{0:T(128)S(1)}, bf16[64,2048]{1,0:T(8,128)(2,1)S(1)}) fusion(bf16[64,2048]{1,0:T(8,128)(2,1)S(1)} %bitcast.55, bf16[2048,2048]{1,0:T(8,128)(2,1)} %param.26, bf16[64,2048]{1,0:T(8,128)(2,1)} %param.18), kind=kOutput, calls=%fused_computation.6 | convolution fusion | flops 537657280 | bytes 9175296 | tf_op jit(solution)/shard_map/dot_general | solution.py:470
  60.3 0.6 reduce-window.6
  60.9 0.2 slice_reduce_fusion
  61.3 0.1 reduce_sum.63
  61.5 0.2 fusion.8
  61.7 0.1 fusion.12
  61.8 0.7 maximum_bitcast_fusion.maps_ref
  62.5 0.8 fusion.4.normed_ref
  63.3 76.3 %experts.1 = bf16[64,2048]{1,0:T(8,128)(2,1)} custom-call(bf16[64,2048]{1,0:T(8,128)(2,1)} %fusion.4.normed_ref, bf16[64,2048]{1,0:T(8,128)(2,1)} %copy-done.1, bf16[4,64,256]{2,1,0:T(8,128)(2,1)} %maximum_bitcast_fusion.maps_ref, bf16[2048,256]{1,0:T(8,128)(2,1)} %bitcast.48, bf16[2048,256]{1,0:T(8,128)(2,1)} %bitcast.50, bf16[256,2048]{1,0:T(8,128)(2,1)} %bitcast.52, ...), custom_call_target="tpu_custom_call" | custom-call | tf_op jit(solution)/shard_map/experts/pallas_call | solution.py:383
  139.7 1.7 %copy.102 = bf16[64,2048]{1,0:T(8,128)(2,1)} copy(bf16[64,2048]{1,0:T(8,128)(2,1)} %experts.1) | data formatting | bytes 524288
  (35 shorter events, 0.9 us)
Async XLA Ops:
  0.0 2.0 %copy-start = (bf16[512,3072]{1,0:T(8,128)(2,1)S(1)}, bf16[512,3072]{1,0:T(8,128)(2,1)}, u32[]{:S(2)}) copy-start(bf16[512,3072]{1,0:T(8,128)(2,1)} %param.24) | copy-start | bytes 9437188
  2.0 11.7 %copy-start.3 = (bf16[128,64]{0,1:T(8,128)(2,1)S(1)}, bf16[128,64]{0,1:T(8,128)(2,1)}, u32[]{:S(2)}) copy-start(bf16[128,64]{0,1:T(8,128)(2,1)} %param.21) | copy-start | bytes 49156
  10.7 7.5 %copy-start.2 = (bf16[128,256]{1,0:T(8,128)(2,1)S(1)}, bf16[128,256]{1,0:T(8,128)(2,1)}, u32[]{:S(2)}) copy-start(bf16[128,256]{1,0:T(8,128)(2,1)} %param.20) | copy-start | bytes 196612
  39.8 13.8 %copy-start.5 = (s32[64,4]{0,1:T(4,128)S(1)}, s32[64,4]{0,1:T(4,128)}, u32[]{:S(2)}) copy-start(s32[64,4]{0,1:T(4,128)} %param.28) | copy-start | bytes 3076
  50.2 5.0 %all-to-all-start = ((bf16[2,64,1024]{2,1,0:T(8,128)(2,1)}), bf16[2,64,1024]{2,1,0:T(8,128)(2,1)S(1)}, u32[]{:S(2)}, u32[]{:S(2)}) async-start(bf16[2,64,1024]{2,1,0:T(8,128)(2,1)} %bitcast.58), calls=%async_computation | async-start | bytes 524288 | tf_op jit(solution)/shard_map/all_to_all | solution.py:469
  55.2 6.4 %copy-start.6 = (f32[64,4]{0,1:T(4,128)S(1)}, f32[64,4]{0,1:T(4,128)}, u32[]{:S(2)}) copy-start(f32[64,4]{0,1:T(4,128)} %param.29) | copy-start | bytes 3076
  55.2 7.3 %copy-start.4 = (f32[2048]{0:T(1024)S(1)}, f32[2048]{0:T(1024)}, u32[]{:S(2)}) copy-start(f32[2048]{0:T(1024)} %param.27) | copy-start | bytes 24580
  60.3 3.0 %copy-start.1 = (bf16[64,2048]{1,0:T(8,128)(2,1)}, bf16[64,2048]{1,0:T(8,128)(2,1)S(1)}, u32[]{:S(2)}) copy-start(bf16[64,2048]{1,0:T(8,128)(2,1)S(1)} %get-tuple-element.22.stream_ref) | copy-start | bytes 786436

commit v2 on v1

--- a/solution.py
+++ b/solution.py
@@ -51,6 +51,14 @@
     return 1
 
 
+def nearest(nz, z, k):
+    place = jnp.int32(0)
+    for at in range(nz):
+        order = sorted(range(nz), key=lambda other: (abs(other - at), other))
+        place = place + jnp.where(z == at, order[k], 0)
+    return place
+
+
 def remote(src, dst, send_sem, recv_sem, sp, tp):
     return pltpu.make_async_remote_copy(
         src_ref=src,
@@ -99,7 +107,7 @@
 
     def across(dz, d):
         b = block_of(dz, 0)
-        src = x_ref.at[t] if dz == 0 else kv_ref.at[b, t]
+        src = x_ref.at[t] if isinstance(dz, int) else kv_ref.at[b, t]
         return remote(
             src, kv_ref.at[b, t], ps.at[dz, d], pr.at[dz, d], z * pn + (p + d) % pn, t
         )
@@ -115,22 +123,25 @@
         remote(u_ref, uo_ref, ws.at[1], wr.at[1], me, 1 - t),
         remote(d_ref, do_ref, ws.at[2], wr.at[2], me, 1 - t),
     ]
-    for dz in range(1, nz):
-        along(dz).start()
+    away = [(nearest(nz, z, k) - z + nz) % nz for k in range(nz)]
+    for k in range(1, nz):
+        along(away[k]).start()
     for d in range(1, pn):
         across(0, d).start()
     for copy in weights:
         copy.start()
     kv_ref[me] = x_ref[...]
-    for dz in range(1, nz):
+    behind = [jnp.int32(0)] + [(z - nearest(nz, z, k) + nz) % nz for k in range(1, nz)]
+    for k in range(1, nz):
+        dz = behind[k]
         along(dz).wait_recv()
         for d in range(1, pn):
             across(dz, d).start()
         swap(dz, 0).start()
-    for dz in range(nz):
-        for d in range(1, pn):
-            across(dz, d).wait_recv()
-            swap(dz, d).start()
+    for k in range(nz):
+        for d in range(1, pn):
+            across(behind[k], d).wait_recv()
+            swap(behind[k], d).start()
     for dz in range(nz):
         for d in range(pn):
             if dz or d:
@@ -178,15 +189,28 @@
 TN = (((0,), (0,)), ((), ()))
 
 
-def attend_kernel(heads, t_ref, qn_ref, qr_ref, w_ref, kv_ref, out_ref):
+def attend_kernel(heads, t_ref, x_ref, cos_ref, sin_ref, wq_ref, w_ref, kv_ref, out_ref):
     latent = kv_ref.shape[1] - LANES
     pair = KEY_PLAIN_WIDTH + VALUE_HEAD_WIDTH
-    rows = qn_ref.shape[1]
+    rows = x_ref.shape[0]
+    scale = (KEY_PLAIN_WIDTH + ROTARY_WIDTH) ** (-0.5)
+    raw = jnp.dot(x_ref[...], wq_ref[...], preferred_element_type=F32) * scale
+    first, middle, last = raw[:, :LANES], raw[:, LANES : 2 * LANES], raw[:, 2 * LANES :]
+    lane = lax.broadcasted_iota(jnp.int32, (rows, LANES), 1)
+    low = lane < ROTARY_WIDTH
+    middle_swapped = pltpu.roll(middle, LANES - ROTARY_WIDTH, 1)
+    last_swapped = pltpu.roll(last, LANES - ROTARY_WIDTH, 1)
+    plain = (first, jnp.where(low, middle_swapped, last_swapped))
+    half = ROTARY_WIDTH // 2
     parts = []
-    for h in range(heads):
+    for h, rotary in enumerate((middle, last_swapped)):
+        other = jnp.where(
+            lane < half, pltpu.roll(rotary, LANES - half, 1), pltpu.roll(rotary, half, 1)
+        )
+        turned = jnp.where(low, rotary * cos_ref[...] + other * sin_ref[...], 0.0).astype(BF16)
         wk = w_ref[:, h * pair : h * pair + KEY_PLAIN_WIDTH]
-        qa = lax.dot_general(qn_ref[h], wk, NT, preferred_element_type=F32).astype(BF16)
-        parts.append(jnp.concatenate([qa, qr_ref[h]], axis=1))
+        qa = lax.dot_general(plain[h].astype(BF16), wk, NT, preferred_element_type=F32)
+        parts.append(jnp.concatenate([qa.astype(BF16), turned], axis=1))
     q = jnp.concatenate(parts, axis=0)
     scores = lax.dot_general(q, kv_ref[...], NT, preferred_element_type=F32)
     weights = jnp.exp(scores - jnp.max(scores, axis=-1, keepdims=True))
@@ -200,18 +224,22 @@
         ).astype(BF16)
 
 
-def attend(tp_index, plain, rotary, weight, kv, heads):
-    local_heads, rows, _ = plain.shape
+def attend(tp_index, query, cos_table, sin_table, query_weight, weight, kv, local_heads):
+    heads = 2
+    rows, rank = query.shape
     steps = local_heads // heads
     pair = KEY_PLAIN_WIDTH + VALUE_HEAD_WIDTH
+    query_block = heads * (KEY_PLAIN_WIDTH + ROTARY_WIDTH)
     return pl.pallas_call(
         functools.partial(attend_kernel, heads),
         grid_spec=pltpu.PrefetchScalarGridSpec(
             num_scalar_prefetch=1,
             grid=(steps,),
             in_specs=[
-                pl.BlockSpec((heads, rows, LANES), lambda i, t: (i, 0, 0)),
-                pl.BlockSpec((heads, rows, LANES), lambda i, t: (i, 0, 0)),
+                pl.BlockSpec((rows, rank), lambda i, t: (0, 0)),
+                pl.BlockSpec((rows, LANES), lambda i, t: (0, 0)),
+                pl.BlockSpec((rows, LANES), lambda i, t: (0, 0)),
+                pl.BlockSpec((rank, query_block), lambda i, t: (0, t[0] * steps + i)),
                 pl.BlockSpec((weight.shape[0], heads * pair), lambda i, t: (0, t[0] * steps + i)),
                 pl.BlockSpec(kv.shape, lambda i, t: (0, 0)),
             ],
@@ -220,7 +248,7 @@
         out_shape=jax.ShapeDtypeStruct((rows, local_heads * VALUE_HEAD_WIDTH), BF16),
         compiler_params=pltpu.CompilerParams(vmem_limit_bytes=60 * 1024 * 1024),
         name="attend",
-    )(tp_index.reshape(1), plain, rotary, weight, kv)
+    )(tp_index.reshape(1), query, cos_table, sin_table, query_weight, weight, kv)
 
 
 def silu(v):
@@ -252,57 +280,70 @@
         copy.start()
     greet(n, nz, False)
 
-    def ahead(dz):
-        return ((z + dz) % nz) * pn + p
-
-    def rows_along(dz):
-        return remote(normed_ref, zb.at[dz], zs.at[dz], zr.at[dz], ahead(dz), t)
+    near = [nearest(nz, z, k) for k in range(nz)]
+
+    def hop(src, b, step):
+        return remote(
+            src, zb.at[b], zs.at[b, (step + 1) // 2], zr.at[b], (z + step) * pn + p, t
+        )
 
     def maps_along(dz):
-        return remote(
-            maps_ref.at[(z + dz) % nz], zm.at[dz], ms.at[dz], mr.at[dz], ahead(dz), t
-        )
-
-    def across(dz, d):
+        to = (z + dz) % nz
+        return remote(maps_ref.at[to], zm.at[z], ms.at[to], mr.at[z], to * pn + p, t)
+
+    def across(b, d):
         q = (p + d) % pn
-        return remote(
-            sb.at[dz, q], ab.at[dz, d], ps.at[dz, d], pr.at[dz, d], z * pn + q, t
-        )
-
-    def back(dz, d):
+        return remote(sb.at[b, q], ab.at[b, d], ps.at[b, d], pr.at[b, d], z * pn + q, t)
+
+    def back(b, d):
         q = (p - d + pn) % pn
-        return remote(
-            ob.at[dz, d], rb.at[dz, p], rs.at[dz, d], rr.at[dz, d], z * pn + q, t
-        )
-
-    def home(dz):
-        return remote(
-            pb.at[dz], qb.at[dz], cs.at[dz], cr.at[dz], ((z - dz + nz) % nz) * pn + p, t
-        )
+        return remote(ob.at[b, d], rb.at[b, p], rs.at[b, d], rr.at[b, d], z * pn + q, t)
+
+    def home(b):
+        return remote(pb.at[b], qb.at[z], cs.at[b], cr.at[z], b * pn + p, t)
+
+    def arrived(b):
+        remote(maps_ref.at[z], zm.at[b], ms.at[z], mr.at[b], b * pn + p, t).wait_recv()
+        remote(normed_ref, zb.at[b], zs.at[b, 0], zr.at[b], b * pn + p, t).wait_recv()
 
     for dz in range(1, nz):
         maps_along(dz).start()
-        rows_along(dz).start()
-    zb[0] = normed_ref[...]
-    zm[0] = maps_ref[z]
-
-    def pick(dz, carried):
-        @pl.when(dz > 0)
+
+    @pl.when(z > 0)
+    def _():
+        hop(normed_ref, z, -1).start()
+
+    @pl.when(z < nz - 1)
+    def _():
+        hop(normed_ref, z, 1).start()
+
+    zb[z] = normed_ref[...]
+    zm[z] = maps_ref[z]
+
+    def pick(b):
+        chosen = lax.dot_general(zm[b][:, :slots], zb[b], TN, preferred_element_type=F32)
+        for q in range(pn):
+            sb[b, q] = chosen[q * cap : (q + 1) * cap].astype(BF16)
+        ab[b, 0] = sb[b, p]
+        for d in range(1, pn):
+            across(b, d).start()
+
+    def take(b):
+        arrived(b)
+
+        @pl.when((b > z) & (z > 0))
         def _():
-            maps_along(dz).wait_recv()
-            rows_along(dz).wait_recv()
-
-        chosen = lax.dot_general(
-            zm[dz][:, :slots], zb[dz], TN, preferred_element_type=F32
-        )
-        for q in range(pn):
-            sb[dz, q] = chosen[q * cap : (q + 1) * cap].astype(BF16)
-        ab[dz, 0] = sb[dz, p]
-        for d in range(1, pn):
-            across(dz, d).start()
-        return carried
-
-    lax.fori_loop(0, nz, pick, 0)
+            hop(zb.at[b], b, -1).start()
+
+        @pl.when((b < z) & (z < nz - 1))
+        def _():
+            hop(zb.at[b], b, 1).start()
+
+        pick(b)
+
+    pick(z)
+    if nz > 1:
+        take(near[1])
     for copy in loads:
         copy.wait()
     normed = normed_ref[...]
@@ -313,16 +354,25 @@
     acc[...] = stream_ref[...].astype(F32) + jnp.dot(
         shared_inner, sd[...], preferred_element_type=F32
     )
+    for k in range(2, nz):
+        take(near[k])
+
+    def turn_of(k):
+        place = jnp.int32(0)
+        for at in range(nz):
+            place = place + jnp.where(k == at, near[(at + 1) % nz], 0)
+        return place
 
     def stack(ref, dz):
         if cap % 16 == 0:
             return ref[dz].reshape(slots, width)
         return jnp.concatenate([ref[dz, d].astype(F32) for d in range(pn)], axis=0).astype(BF16)
 
-    def expert(dz, carried):
-        for d in range(1, pn):
-            across(dz, d).wait_recv()
-        rows = stack(ab, dz)
+    def expert(k, carried):
+        b = turn_of(k)
+        for d in range(1, pn):
+            across(b, d).wait_recv()
+        rows = stack(ab, b)
         halves = []
         for h in range(2):
             gate_act = jnp.dot(rows, wg[h], preferred_element_type=F32)
@@ -331,44 +381,59 @@
             halves.append(jnp.dot(inner, wd[h], preferred_element_type=F32).astype(BF16))
         summed = halves[0].astype(F32) + halves[1].astype(F32)
         for d in range(pn):
-            ob[dz, d] = summed[d * cap : (d + 1) * cap].astype(BF16)
-        rb[dz, p] = ob[dz, 0]
-        for d in range(1, pn):
-            back(dz, d).start()
+            ob[b, d] = summed[d * cap : (d + 1) * cap].astype(BF16)
+        rb[b, p] = ob[b, 0]
+        for d in range(1, pn):
+            back(b, d).start()
         return carried
 
     lax.fori_loop(0, nz, expert, 0)
 
-    def combine(dz, carried):
-        for d in range(1, pn):
-            back(dz, d).wait_recv()
-        part = jnp.dot(zm[dz][:, slots:], stack(rb, dz), preferred_element_type=F32)
-
-        @pl.when(dz == 0)
-        def _():
-            acc[...] += part
-
-        @pl.when(dz > 0)
-        def _():
-            pb[dz] = part.astype(BF16)
-            home(dz).start()
-
+    def returned(b):
+        for d in range(1, pn):
+            back(b, d).wait_recv()
+        return jnp.dot(zm[b][:, slots:], stack(rb, b), preferred_element_type=F32)
+
+    def combine(k, carried):
+        b = turn_of(k)
+        pb[b] = returned(b).astype(BF16)
+        home(b).start()
         return carried
 
-    lax.fori_loop(0, nz, combine, 0)
-    total = acc[...]
-    for dz in range(1, nz):
-        home(dz).wait_recv()
-        total = total + qb[dz].astype(F32)
+    lax.fori_loop(0, nz - 1, combine, 0)
+    total = acc[...] + returned(z)
+    for k in range(1, nz):
+        b = near[k]
+        remote(pb.at[b], qb.at[b], cs.at[b], cr.at[b], b * pn + p, t).wait_recv()
+        total = total + qb[b].astype(F32)
     out_ref[...] = total.astype(BF16)
     for dz in range(1, nz):
         maps_along(dz).wait_send()
-        rows_along(dz).wait_send()
-        home(dz).wait_send()
-    for dz in range(nz):
-        for d in range(1, pn):
-            across(dz, d).wait_send()
-            back(dz, d).wait_send()
+
+    @pl.when(z > 0)
+    def _():
+        hop(normed_ref, z, -1).wait_send()
+
+    @pl.when(z < nz - 1)
+    def _():
+        hop(normed_ref, z, 1).wait_send()
+
+    for k in range(1, nz):
+        b = near[k]
+        home(b).wait_send()
+
+        @pl.when((b > z) & (z > 0))
+        def _():
+            hop(zb.at[b], b, -1).wait_send()
+
+        @pl.when((b < z) & (z < nz - 1))
+        def _():
+            hop(zb.at[b], b, 1).wait_send()
+
+    for b in range(nz):
+        for d in range(1, pn):
+            across(b, d).wait_send()
+            back(b, d).wait_send()
 
 
 def experts(n, nz, cap, normed, stream, maps, weights, shared):
@@ -402,7 +467,7 @@
             pltpu.VMEM((nz, rows, width), BF16),
             pltpu.VMEM((rows, width), F32),
             dma((9,)),
-            dma((nz,)), dma((nz,)), dma((nz,)), dma((nz,)),
+            dma((nz, 2)), dma((nz,)), dma((nz,)), dma((nz,)),
             dma((nz, pn)), dma((nz, pn)), dma((nz, pn)), dma((nz, pn)),
             dma((nz,)), dma((nz,)),
         ],
@@ -454,17 +519,13 @@
     kv = kv.reshape(n * tok_rows, packed.shape[1])
 
     query_normed = rms_scale(query_compressed, query_norm_gain).astype(BF16)
-    query_cols = lax.dynamic_slice_in_dim(
-        query_up_weight, tp_index * local_heads * head_width, local_heads * head_width, 1
-    )
-    raw_query = jnp.dot(query_normed, query_cols, preferred_element_type=F32) * head_width ** (-0.5)
-    raw_query = raw_query.reshape(tok_rows, local_heads, head_width)
-    turned = turn(raw_query[:, :, KEY_PLAIN_WIDTH:], cos_part[:, None, :], sine_part[:, None, :])
-    plain = jnp.transpose(raw_query[:, :, :KEY_PLAIN_WIDTH].astype(BF16), (1, 0, 2))
-    rotary = jnp.transpose(
-        jnp.pad(turned.astype(BF16), ((0, 0), (0, 0), (0, LANES - ROTARY_WIDTH))), (1, 0, 2)
-    )
-    local_out = attend(tp_index, plain, rotary, keyvalue_up_weight, kv, 2)
+    blank = jnp.zeros((tok_rows, LANES - ROTARY_WIDTH), F32)
+    cos_table = jnp.concatenate([cos_part, cos_part, blank], axis=1)
+    sin_table = jnp.concatenate([-sine_part, sine_part, blank], axis=1)
+    local_out = attend(
+        tp_index, query_normed, cos_table, sin_table, query_up_weight, keyvalue_up_weight, kv,
+        local_heads,
+    )
 
     attended = lax.all_to_all(local_out, "tp", split_axis=0, concat_axis=1, tiled=True)
     projected = jnp.dot(attended, out_proj, preferred_element_type=F32)

time: 142 us -> 119 us (0.84)
  Pallas kernels: 107 us -> 96.3 us
  local copies, waits for them, and re-layouts: 12.5 us -> 3.37 us
  matrix products: 7.34 us -> 5.11 us
    pallas_call x1, Pallas kernels: 76.3 us -> 65.2 us  [experts(): pl.pallas_call(functools.partial(moe_kernel, n, nz, cap), out_shape=jax.S...]
    unnamed x19 -> x13, local copies, waits for them, and re-layouts: 6.37 us -> 2.62 us
    mul x1 -> x0, local copies, waits for them, and re-layouts: 2.28 us -> none  [shards(): jnp.dot(query_normed, query_cols, preferred_element_type=F32)]
    dot_general x1 -> x0, matrix products: 2.25 us -> none  [shards(): jnp.dot(query_normed, query_cols, preferred_element_type=F32)]
    another operation x4 -> x3, other arithmetic: 2.8 us -> 0.95 us
    convert_element_type x0 -> x1, other arithmetic: none -> 1.66 us  [shards(): query_normed = rms_scale(query_compressed, query_norm_gain).astype(BF16)]
    split x1 -> x0, local copies, waits for them, and re-layouts: 1.64 us -> none  [turn(): lower_half, upper_half = jnp.split(values, 2, axis=-1)]
where the time goes in v2:
time: 119 us
  Pallas kernels  96.3 us (81%)
  other arithmetic  8.97 us (8%)
  matrix products  5.11 us (4%)
  starting transfers between devices  3.44 us (3%)
  local copies, waits for them, and re-layouts  3.37 us (3%)
  waiting for transfers between devices  1.22 us (1%)
    pallas_call x1, Pallas kernels, experts(): pl.pallas_call(functools.partial(moe_kernel, n, nz, cap), out_shape=jax.S...  65.2 us
    pallas_call x1, Pallas kernels, gather_latents(): pl.pallas_call(functools.partial(gather_kernel, n, nz), out_shape=(jax.Sh...  19.7 us
    pallas_call x1, Pallas kernels, attend(): pl.pallas_call(functools.partial(attend_kernel, heads), grid_spec=pltpu.P...  11.3 us
    dot_general x1, matrix products, shards(): projected = jnp.dot(attended, out_proj, preferred_element_type=F32)  5.11 us
    all_to_all x1, starting transfers between devices, shards(): lax.all_to_all(local_out, 'tp', split_axis=0, concat_axis=1, tiled=True)  3.44 us
    unnamed x13, local copies, waits for them, and re-layouts  2.62 us
  transfers between devices with their start and end apart: 1, of which 1 were waited for; matrix products, arithmetic and copies ran while one was open for 0% of the time, Pallas kernels for 0%

profile of v2, /device:TPU:0, one launch (start us, length us, event | category | flops | bytes accessed | tf_op | source)
XLA Modules:
  0.0 118.6 jit_solution(13948498523807827141)
XLA Ops:
  0.0 0.8 copy.53
  0.9 0.9 fusion.10
  1.8 1.0 fusion.6
  2.9 0.9 fusion.12
  3.8 0.1 pad.5.clone
  3.9 0.1 pad.11.clone
  4.0 1.7 %fusion.8.x_ref = bf16[128,512]{1,0:T(8,128)(2,1)} fusion(bf16[128,512]{1,0:T(8,128)(2,1)} %param.19, f32[512]{0:T(512)} %param.22, f32[128]{0:T(128)S(1)} %add_rsqrt_fusion.2), kind=kLoop, calls=%fused_computation.14 | loop fusion | flops 262144 | bytes 264704 | tf_op jit(solution)/shard_map/convert_element_type | solution.py:521
  5.6 0.3 fusion.17
  6.0 0.7 maximum_maximum_fusion
  6.7 19.7 %gather_latents.1 = (bf16[16,2,64,384]{3,2,1,0:T(8,128)(2,1)}, bf16[2048,256]{1,0:T(8,128)(2,1)}, bf16[2048,256]{1,0:T(8,128)(2,1)}, bf16[256,2048]{1,0:T(8,128)(2,1)}) custom-call(bf16[2,64,384]{2,1,0:T(8,128)(2,1)} %bitcast.53, bf16[2048,256]{1,0:T(8,128)(2,1)} %bitcast.43, bf16[2048,256]{1,0:T(8,128)(2,1)} %bitcast.45, bf16[256,2048]{1,0:T(8,128)(2,1)} %bitcast.47), custom_call_target="tpu_custom_call" | custom-call | tf_op jit(solution)/shard_map/gather_latents/pallas_call | solution.py:163
  26.4 0.8 maximum_maximum_fusion.2
  27.2 11.3 %attend.1 = bf16[128,1024]{1,0:T(8,128)(2,1)} custom-call(s32[1]{0:T(128)} %bitcast.t_ref, bf16[128,512]{1,0:T(8,128)(2,1)} %fusion.8.x_ref, f32[128,128]{1,0:T(8,128)} %get-tuple-element.19.cos_ref, f32[128,128]{1,0:T(8,128)} %get-tuple-element.18.sin_ref, bf16[512,3072]{1,0:T(8,128)(2,1)} %wq_ref.1, bf16[256,4096]{1,0:T(8,128)(2,1)} %w_ref.1, ...), custom_call_target="tpu_custom_call" | custom-call | tf_op jit(solution)/shard_map/attend/pallas_call | solution.py:233
  38.5 3.4 %all-to-all-start = ((bf16[2,64,1024]{2,1,0:T(8,128)(2,1)}), bf16[2,64,1024]{2,1,0:T(8,128)(2,1)S(1)}, u32[]{:S(2)}, u32[]{:S(2)}) async-start(bf16[2,64,1024]{2,1,0:T(8,128)(2,1)} %bitcast.52), calls=%async_computation | async-start | bytes 524288 | tf_op jit(solution)/shard_map/all_to_all | solution.py:530
  42.0 0.0 copy-done.3
  42.0 0.1 copy.55
  42.1 0.1 eq.43
  42.2 0.1 eq.39
  42.3 1.2 %all-to-all-done = bf16[2,64,1024]{2,1,0:T(8,128)(2,1)S(1)} async-done(((bf16[2,64,1024]{2,1,0:T(8,128)(2,1)}), bf16[2,64,1024]{2,1,0:T(8,128)(2,1)S(1)}, u32[]{:S(2)}, u32[]{:S(2)}) %all-to-all-start) | async-done | bytes 262176 | tf_op jit(solution)/shard_map/all_to_all | solution.py:530
  43.5 0.0 copy-start.4
  43.5 0.0 copy-start.2
  43.6 5.1 %fusion.1 = (f32[64]{0:T(128)S(1)}, bf16[64,2048]{1,0:T(8,128)(2,1)S(1)}) fusion(bf16[64,2048]{1,0:T(8,128)(2,1)S(1)} %bitcast.49, bf16[2048,2048]{1,0:T(8,128)(2,1)} %param.26, bf16[64,2048]{1,0:T(8,128)(2,1)S(1)} %copy-done.1), kind=kOutput, calls=%fused_computation.4 | convolution fusion | flops 537657280 | bytes 9175296 | tf_op jit(solution)/shard_map/dot_general | solution.py:531
  48.7 0.6 reduce-window.6
  49.3 0.2 slice_reduce_fusion
  49.5 0.1 fusion.22
  49.6 0.1 reduce_sum.63
  49.7 0.1 copy.58
  49.9 0.1 fusion.5
  50.0 0.1 fusion.9
  50.2 0.7 maximum_bitcast_fusion.maps_ref
  50.8 0.8 fusion.3.normed_ref
  51.7 65.2 %experts.1 = bf16[64,2048]{1,0:T(8,128)(2,1)} custom-call(bf16[64,2048]{1,0:T(8,128)(2,1)} %fusion.3.normed_ref, bf16[64,2048]{1,0:T(8,128)(2,1)} %copy-done, bf16[4,64,256]{2,1,0:T(8,128)(2,1)} %maximum_bitcast_fusion.maps_ref, bf16[2048,256]{1,0:T(8,128)(2,1)} %bitcast.44, bf16[2048,256]{1,0:T(8,128)(2,1)} %bitcast.46, bf16[256,2048]{1,0:T(8,128)(2,1)} %bitcast.48, ...), custom_call_target="tpu_custom_call" | custom-call | tf_op jit(solution)/shard_map/experts/pallas_call | solution.py:448
  116.9 1.7 %copy.69 = bf16[64,2048]{1,0:T(8,128)(2,1)} copy(bf16[64,2048]{1,0:T(8,128)(2,1)} %experts.1) | data formatting | bytes 524288
  (23 shorter events, 0.2 us)
Async XLA Ops:
  27.2 14.8 %copy-start.3 = (s32[64,4]{0,1:T(4,128)S(1)}, s32[64,4]{0,1:T(4,128)}, u32[]{:S(2)}) copy-start(s32[64,4]{0,1:T(4,128)} %param.28) | copy-start | bytes 3076
  27.2 16.3 %copy-start.1 = (bf16[64,2048]{1,0:T(8,128)(2,1)S(1)}, bf16[64,2048]{1,0:T(8,128)(2,1)}, u32[]{:S(2)}) copy-start(bf16[64,2048]{1,0:T(8,128)(2,1)} %param.18) | copy-start | bytes 786436
  38.5 5.0 %all-to-all-start = ((bf16[2,64,1024]{2,1,0:T(8,128)(2,1)}), bf16[2,64,1024]{2,1,0:T(8,128)(2,1)S(1)}, u32[]{:S(2)}, u32[]{:S(2)}) async-start(bf16[2,64,1024]{2,1,0:T(8,128)(2,1)} %bitcast.52), calls=%async_computation | async-start | bytes 524288 | tf_op jit(solution)/shard_map/all_to_all | solution.py:530
  43.5 6.3 %copy-start.4 = (f32[64,4]{0,1:T(4,128)S(1)}, f32[64,4]{0,1:T(4,128)}, u32[]{:S(2)}) copy-start(f32[64,4]{0,1:T(4,128)} %param.29) | copy-start | bytes 3076
  43.5 7.3 %copy-start.2 = (f32[2048]{0:T(1024)S(1)}, f32[2048]{0:T(1024)}, u32[]{:S(2)}) copy-start(f32[2048]{0:T(1024)} %param.27) | copy-start | bytes 24580
  48.7 3.0 %copy-start = (bf16[64,2048]{1,0:T(8,128)(2,1)}, bf16[64,2048]{1,0:T(8,128)(2,1)S(1)}, u32[]{:S(2)}) copy-start(bf16[64,2048]{1,0:T(8,128)(2,1)S(1)} %get-tuple-element.21.stream_ref) | copy-start | bytes 786436

commit v3 on v2

--- a/solution.py
+++ b/solution.py
@@ -257,16 +257,25 @@
 
 def moe_kernel(
     n, nz, cap,
-    normed_ref, stream_ref, maps_ref, g_ref, u_ref, d_ref, go_ref, uo_ref, do_ref,
-    sg_ref, su_ref, sd_ref, out_ref,
-    wg, wu, wd, sg, su, sd, zb, zm, sb, ab, ob, rb, pb, qb, acc,
-    ls, zs, zr, ms, mr, ps, pr, rs, rr, cs, cr,
+    local_ref, stream_in_ref, gain_ref, maps_ref, g_ref, u_ref, d_ref, go_ref, uo_ref, do_ref,
+    sg_ref, su_ref, sd_ref, proj_ref, out_ref,
+    wg, wu, wd, sg, su, sd, proj, other, zb, zm, sb, ab, ob, rb, pb, qb, acc,
+    ls, hs, hr, zs, zr, ms, mr, ps, pr, rs, rr, cs, cr,
 ):
     pn = n // nz
     slots = pn * cap
-    width = normed_ref.shape[1]
+    width = stream_in_ref.shape[1]
+    cols = local_ref.shape[2]
     me, t = lax.axis_index("sp"), lax.axis_index("tp")
     z, p = me // pn, me % pn
+    mine = pl.ds(pl.multiple_of(t * cols, LANES), cols)
+    theirs = pl.ds(pl.multiple_of((1 - t) * cols, LANES), cols)
+    proj_loads = [
+        pltpu.make_async_copy(proj_ref.at[part], proj.at[part], ls.at[9 + i])
+        for i, part in enumerate((mine, theirs))
+    ]
+    for copy in proj_loads:
+        copy.start()
     loads = [
         pltpu.make_async_copy(src, dst, ls.at[i])
         for i, (src, dst) in enumerate(
@@ -278,7 +287,9 @@
     ]
     for copy in loads:
         copy.start()
-    greet(n, nz, False)
+    greet(n, nz, True)
+    exchange = remote(local_ref.at[1 - t], other, hs.at[0], hr.at[0], me, 1 - t)
+    exchange.start()
 
     near = [nearest(nz, z, k) for k in range(nz)]
 
@@ -304,21 +315,27 @@
 
     def arrived(b):
         remote(maps_ref.at[z], zm.at[b], ms.at[z], mr.at[b], b * pn + p, t).wait_recv()
-        remote(normed_ref, zb.at[b], zs.at[b, 0], zr.at[b], b * pn + p, t).wait_recv()
+        remote(zb.at[b], zb.at[b], zs.at[b, 0], zr.at[b], b * pn + p, t).wait_recv()
 
     for dz in range(1, nz):
         maps_along(dz).start()
+    zm[z] = maps_ref[z]
+    proj_loads[0].wait()
+    projected = jnp.dot(local_ref[t], proj[mine], preferred_element_type=F32)
+    exchange.wait()
+    proj_loads[1].wait()
+    projected = projected + jnp.dot(other[...], proj[theirs], preferred_element_type=F32)
+    stream = (stream_in_ref[...].astype(F32) + projected).astype(BF16).astype(F32)
+    acc[...] = stream
+    zb[z] = rms_scale(stream, gain_ref[...]).astype(BF16)
 
     @pl.when(z > 0)
     def _():
-        hop(normed_ref, z, -1).start()
+        hop(zb.at[z], z, -1).start()
 
     @pl.when(z < nz - 1)
     def _():
-        hop(normed_ref, z, 1).start()
-
-    zb[z] = normed_ref[...]
-    zm[z] = maps_ref[z]
+        hop(zb.at[z], z, 1).start()
 
     def pick(b):
         chosen = lax.dot_general(zm[b][:, :slots], zb[b], TN, preferred_element_type=F32)
@@ -346,14 +363,12 @@
         take(near[1])
     for copy in loads:
         copy.wait()
-    normed = normed_ref[...]
+    normed = zb[z]
     shared_inner = (
         silu(jnp.dot(normed, sg[...], preferred_element_type=F32))
         * jnp.dot(normed, su[...], preferred_element_type=F32)
     ).astype(BF16)
-    acc[...] = stream_ref[...].astype(F32) + jnp.dot(
-        shared_inner, sd[...], preferred_element_type=F32
-    )
+    acc[...] += jnp.dot(shared_inner, sd[...], preferred_element_type=F32)
     for k in range(2, nz):
         take(near[k])
 
@@ -412,11 +427,11 @@
 
     @pl.when(z > 0)
     def _():
-        hop(normed_ref, z, -1).wait_send()
+        hop(zb.at[z], z, -1).wait_send()
 
     @pl.when(z < nz - 1)
     def _():
-        hop(normed_ref, z, 1).wait_send()
+        hop(zb.at[z], z, 1).wait_send()
 
     for k in range(1, nz):
         b = near[k]
@@ -436,9 +451,10 @@
             back(b, d).wait_send()
 
 
-def experts(n, nz, cap, normed, stream, maps, weights, shared):
+def experts(n, nz, cap, local_out, stream_in, gain, maps, weights, shared, out_proj):
     pn = n // nz
-    rows, width = normed.shape
+    rows, width = stream_in.shape
+    cols = local_out.shape[1]
     hidden = weights[0].shape[1]
     shared_hidden = shared[0].shape[1]
     anywhere = pl.BlockSpec(memory_space=pl.ANY)
@@ -448,7 +464,7 @@
     return pl.pallas_call(
         functools.partial(moe_kernel, n, nz, cap),
         out_shape=jax.ShapeDtypeStruct((rows, width), BF16),
-        in_specs=[inside] * 3 + [anywhere] * 9,
+        in_specs=[inside] * 4 + [anywhere] * 10,
         out_specs=inside,
         scratch_shapes=[
             pltpu.VMEM((2, width, hidden), BF16),
@@ -457,6 +473,8 @@
             pltpu.VMEM((width, shared_hidden), BF16),
             pltpu.VMEM((width, shared_hidden), BF16),
             pltpu.VMEM((shared_hidden, width), BF16),
+            pltpu.VMEM(out_proj.shape, BF16),
+            pltpu.VMEM((rows, cols), BF16),
             pltpu.VMEM((nz, rows, width), BF16),
             pltpu.VMEM((nz, rows, maps.shape[2]), BF16),
             pltpu.VMEM(plane, BF16),
@@ -466,7 +484,7 @@
             pltpu.VMEM((nz, rows, width), BF16),
             pltpu.VMEM((nz, rows, width), BF16),
             pltpu.VMEM((rows, width), F32),
-            dma((9,)),
+            dma((11,)), dma((1,)), dma((1,)),
             dma((nz, 2)), dma((nz,)), dma((nz,)), dma((nz,)),
             dma((nz, pn)), dma((nz, pn)), dma((nz, pn)), dma((nz, pn)),
             dma((nz,)), dma((nz,)),
@@ -475,7 +493,10 @@
             collective_id=1, has_side_effects=True, vmem_limit_bytes=60 * 1024 * 1024
         ),
         name="experts",
-    )(normed, stream, maps, *weights, *shared)
+    )(
+        local_out.reshape(2, rows, cols), stream_in, gain.reshape(1, width), maps,
+        *weights, *shared, out_proj,
+    )
 
 
 def shards(
@@ -527,11 +548,6 @@
         local_heads,
     )
 
-    attended = lax.all_to_all(local_out, "tp", split_axis=0, concat_axis=1, tiled=True)
-    projected = jnp.dot(attended, out_proj, preferred_element_type=F32)
-    stream = (stream_in.astype(F32) + projected).astype(BF16)
-    normed = rms_scale(stream, ffn_gain).astype(BF16)
-
     shares = (
         routed_scale * expert_weights / jnp.sum(expert_weights, axis=-1, keepdims=True)
     ).astype(BF16)
@@ -555,9 +571,10 @@
     ).reshape(moe_rows, nz, slots)
     maps = jnp.transpose(jnp.concatenate([sender_map, share_map], axis=2), (1, 0, 2))
     return experts(
-        n, nz, capacity, normed, stream, maps,
+        n, nz, capacity, local_out, stream_in, ffn_gain, maps,
         (expert_gate[0], expert_up[0], expert_down[0], gate_other, up_other, down_other),
         (shared_gate, shared_up, shared_down),
+        out_proj,
     )
 
 

time: 119 us -> 109 us (0.916)
  matrix products: 5.11 us -> 0 us
  starting transfers between devices: 3.44 us -> 0 us
  Pallas kernels: 96.3 us -> 99.1 us
  other arithmetic: 8.97 us -> 6.36 us
  waiting for transfers between devices: 1.22 us -> 0 us
    dot_general x1 -> x0, matrix products: 5.11 us -> none  [shards(): projected = jnp.dot(attended, out_proj, preferred_element_type=F32)]
    all_to_all x1 -> x0, starting transfers between devices: 3.44 us -> none  [shards(): lax.all_to_all(local_out, 'tp', split_axis=0, concat_axis=1, tiled=True)]
    pallas_call x1, Pallas kernels: 65.2 us -> 68.1 us  [experts(): pl.pallas_call(functools.partial(moe_kernel, n, nz, cap), out_shape=jax.S...]
    all_to_all x1 -> x0, waiting for transfers between devices: 1.22 us -> none  [shards(): lax.all_to_all(local_out, 'tp', split_axis=0, concat_axis=1, tiled=True)]
    unnamed x13 -> x11, local copies, waits for them, and re-layouts: 2.62 us -> 2.61 us
  transfers between devices with their start and end apart: 1 -> 0, of which waited for: 1 -> 0; matrix products, arithmetic and copies ran while one was open for 0% -> 0% of each run, Pallas kernels for 0% -> 0%
where the time goes in v3:
time: 109 us
  Pallas kernels  99.1 us (91%)
  other arithmetic  6.36 us (6%)
  local copies, waits for them, and re-layouts  3.34 us (3%)
    pallas_call x1, Pallas kernels, experts(): pl.pallas_call(functools.partial(moe_kernel, n, nz, cap), out_shape=jax.S...  68.1 us
    pallas_call x1, Pallas kernels, gather_latents(): pl.pallas_call(functools.partial(gather_kernel, n, nz), out_shape=(jax.Sh...  19.7 us
    pallas_call x1, Pallas kernels, attend(): pl.pallas_call(functools.partial(attend_kernel, heads), grid_spec=pltpu.P...  11.3 us
    unnamed x11, local copies, waits for them, and re-layouts  2.61 us

profile of v3, /device:TPU:0, one launch (start us, length us, event | category | flops | bytes accessed | tf_op | source)
XLA Modules:
  0.0 109.0 jit_solution(1141992713786537934)
XLA Ops:
  0.0 0.8 copy.41
  0.9 0.3 fusion.13
  1.2 0.0 copy-start
  1.2 0.0 copy-start.3
  1.2 1.0 fusion.6
  2.2 0.9 fusion.8
  3.2 0.1 pad.5.clone
  3.2 0.7 maximum_maximum_fusion
  4.0 19.7 %gather_latents.1 = (bf16[16,2,64,384]{3,2,1,0:T(8,128)(2,1)}, bf16[2048,256]{1,0:T(8,128)(2,1)}, bf16[2048,256]{1,0:T(8,128)(2,1)}, bf16[256,2048]{1,0:T(8,128)(2,1)}) custom-call(bf16[2,64,384]{2,1,0:T(8,128)(2,1)} %bitcast.47, bf16[2048,256]{1,0:T(8,128)(2,1)} %bitcast.39, bf16[2048,256]{1,0:T(8,128)(2,1)} %bitcast.41, bf16[256,2048]{1,0:T(8,128)(2,1)} %bitcast.43), custom_call_target="tpu_custom_call" | custom-call | tf_op jit(solution)/shard_map/gather_latents/pallas_call | solution.py:163
  23.7 0.1 pad.11.clone
  23.8 0.8 maximum_maximum_fusion.2
  24.5 0.0 copy-done
  24.5 0.1 fusion.2
  24.7 0.0 copy-done.3
  24.7 0.8 fusion.4.x_ref
  25.4 0.0 copy-start.2
  25.4 11.3 %attend.1 = bf16[128,1024]{1,0:T(8,128)(2,1)} custom-call(s32[1]{0:T(128)} %bitcast.t_ref, bf16[128,512]{1,0:T(8,128)(2,1)} %fusion.4.x_ref, f32[128,128]{1,0:T(8,128)} %get-tuple-element.19.cos_ref, f32[128,128]{1,0:T(8,128)} %get-tuple-element.18.sin_ref, bf16[512,3072]{1,0:T(8,128)(2,1)} %wq_ref.1, bf16[256,4096]{1,0:T(8,128)(2,1)} %w_ref.1, ...), custom_call_target="tpu_custom_call" | custom-call | tf_op jit(solution)/shard_map/attend/pallas_call | solution.py:233
  36.7 0.0 copy-done.1
  36.7 0.1 copy.42
  36.8 0.1 eq.43
  36.9 0.6 reduce-window.6
  37.5 0.2 slice_reduce_fusion
  37.8 0.1 eq.39
  37.9 0.1 fusion.18
  38.0 0.1 reduce_sum.53
  38.1 0.1 copy.45
  38.2 0.0 copy-done.2
  38.2 0.1 fusion.5
  38.4 0.1 fusion.1
  38.5 0.7 maximum_bitcast_fusion.maps_ref
  39.2 68.1 %experts.1 = bf16[64,2048]{1,0:T(8,128)(2,1)} custom-call(bf16[2,64,1024]{2,1,0:T(8,128)(2,1)} %bitcast.46, bf16[64,2048]{1,0:T(8,128)(2,1)} %stream_in_ref.1, f32[1,2048]{1,0:T(1,128)} %bitcast.48, bf16[4,64,256]{2,1,0:T(8,128)(2,1)} %maximum_bitcast_fusion.maps_ref, bf16[2048,256]{1,0:T(8,128)(2,1)} %bitcast.40, bf16[2048,256]{1,0:T(8,128)(2,1)} %bitcast.42, ...), custom_call_target="tpu_custom_call" | custom-call | tf_op jit(solution)/shard_map/experts/pallas_call | solution.py:464
  107.3 1.7 %copy.55 = bf16[64,2048]{1,0:T(8,128)(2,1)} copy(bf16[64,2048]{1,0:T(8,128)(2,1)} %experts.1) | data formatting | bytes 524288
  (15 shorter events, 0.2 us)
Async XLA Ops:
  1.2 23.3 %copy-start = (bf16[128,512]{1,0:T(8,128)(2,1)S(1)}, bf16[128,512]{1,0:T(8,128)(2,1)}, u32[]{:S(2)}) copy-start(bf16[128,512]{1,0:T(8,128)(2,1)} %param.19) | copy-start | bytes 393220
  1.2 23.5 %copy-start.3 = (f32[512]{0:T(512)S(1)}, f32[512]{0:T(512)}, u32[]{:S(2)}) copy-start(f32[512]{0:T(512)} %param.22) | copy-start | bytes 6148
  25.4 11.3 %copy-start.1 = (s32[64,4]{0,1:T(4,128)S(1)}, s32[64,4]{0,1:T(4,128)}, u32[]{:S(2)}) copy-start(s32[64,4]{0,1:T(4,128)} %param.28) | copy-start | bytes 3076
  25.4 12.7 %copy-start.2 = (f32[64,4]{0,1:T(4,128)S(1)}, f32[64,4]{0,1:T(4,128)}, u32[]{:S(2)}) copy-start(f32[64,4]{0,1:T(4,128)} %param.29) | copy-start | bytes 3076

commit v4 on v3

--- a/solution.py
+++ b/solution.py
@@ -369,9 +369,6 @@
         * jnp.dot(normed, su[...], preferred_element_type=F32)
     ).astype(BF16)
     acc[...] += jnp.dot(shared_inner, sd[...], preferred_element_type=F32)
-    for k in range(2, nz):
-        take(near[k])
-
     def turn_of(k):
         place = jnp.int32(0)
         for at in range(nz):
@@ -383,8 +380,7 @@
             return ref[dz].reshape(slots, width)
         return jnp.concatenate([ref[dz, d].astype(F32) for d in range(pn)], axis=0).astype(BF16)
 
-    def expert(k, carried):
-        b = turn_of(k)
+    def expert(b):
         for d in range(1, pn):
             across(b, d).wait_recv()
         rows = stack(ab, b)
@@ -398,11 +394,21 @@
         for d in range(pn):
             ob[b, d] = summed[d * cap : (d + 1) * cap].astype(BF16)
         rb[b, p] = ob[b, 0]
+
+    def give(b):
         for d in range(1, pn):
             back(b, d).start()
-        return carried
-
-    lax.fori_loop(0, nz, expert, 0)
+
+    expert(z)
+    for k in range(2, nz):
+        if k > 2:
+            expert(near[k - 2])
+        take(near[k])
+    for k in range(1, nz):
+        if k > max(nz - 3, 0):
+            expert(near[k])
+        give(near[k])
+    give(z)
 
     def returned(b):
         for d in range(1, pn):

time: 109 us -> 110 us (level)
  no operation moved by 1% of the time
where the time goes in v4:
time: 110 us; the launch traced here: 109 us
  Pallas kernels  99.2 us (90%)
  other arithmetic  6.36 us (6%)
  local copies, waits for them, and re-layouts  3.34 us (3%)
    pallas_call x1, Pallas kernels, experts(): pl.pallas_call(functools.partial(moe_kernel, n, nz, cap), out_shape=jax.S...  68.2 us
    pallas_call x1, Pallas kernels, gather_latents(): pl.pallas_call(functools.partial(gather_kernel, n, nz), out_shape=(jax.Sh...  19.7 us
    pallas_call x1, Pallas kernels, attend(): pl.pallas_call(functools.partial(attend_kernel, heads), grid_spec=pltpu.P...  11.3 us
    unnamed x11, local copies, waits for them, and re-layouts  2.61 us

profile of v4, /device:TPU:0, one launch (start us, length us, event | category | flops | bytes accessed | tf_op | source)
XLA Modules:
  0.0 109.1 jit_solution(2923003364194922833)
XLA Ops:
  0.0 0.8 copy.41
  0.9 0.3 fusion.13
  1.2 0.0 copy-start
  1.2 0.0 copy-start.3
  1.2 1.0 fusion.6
  2.2 0.9 fusion.8
  3.2 0.1 pad.5.clone
  3.2 0.7 maximum_maximum_fusion
  4.0 19.7 %gather_latents.1 = (bf16[16,2,64,384]{3,2,1,0:T(8,128)(2,1)}, bf16[2048,256]{1,0:T(8,128)(2,1)}, bf16[2048,256]{1,0:T(8,128)(2,1)}, bf16[256,2048]{1,0:T(8,128)(2,1)}) custom-call(bf16[2,64,384]{2,1,0:T(8,128)(2,1)} %bitcast.47, bf16[2048,256]{1,0:T(8,128)(2,1)} %bitcast.39, bf16[2048,256]{1,0:T(8,128)(2,1)} %bitcast.41, bf16[256,2048]{1,0:T(8,128)(2,1)} %bitcast.43), custom_call_target="tpu_custom_call" | custom-call | tf_op jit(solution)/shard_map/gather_latents/pallas_call | solution.py:163
  23.7 0.1 pad.11.clone
  23.8 0.8 maximum_maximum_fusion.2
  24.5 0.0 copy-done
  24.5 0.1 fusion.2
  24.7 0.0 copy-done.3
  24.7 0.8 fusion.4.x_ref
  25.4 0.0 copy-start.2
  25.4 11.3 %attend.1 = bf16[128,1024]{1,0:T(8,128)(2,1)} custom-call(s32[1]{0:T(128)} %bitcast.t_ref, bf16[128,512]{1,0:T(8,128)(2,1)} %fusion.4.x_ref, f32[128,128]{1,0:T(8,128)} %get-tuple-element.19.cos_ref, f32[128,128]{1,0:T(8,128)} %get-tuple-element.18.sin_ref, bf16[512,3072]{1,0:T(8,128)(2,1)} %wq_ref.1, bf16[256,4096]{1,0:T(8,128)(2,1)} %w_ref.1, ...), custom_call_target="tpu_custom_call" | custom-call | tf_op jit(solution)/shard_map/attend/pallas_call | solution.py:233
  36.7 0.0 copy-done.1
  36.7 0.1 copy.42
  36.8 0.1 eq.43
  36.9 0.6 reduce-window.6
  37.5 0.2 slice_reduce_fusion
  37.8 0.1 eq.39
  37.9 0.1 fusion.18
  38.0 0.1 reduce_sum.53
  38.1 0.1 copy.45
  38.2 0.0 copy-done.2
  38.2 0.1 fusion.5
  38.4 0.1 fusion.1
  38.5 0.7 maximum_bitcast_fusion.maps_ref
  39.2 68.2 %experts.1 = bf16[64,2048]{1,0:T(8,128)(2,1)} custom-call(bf16[2,64,1024]{2,1,0:T(8,128)(2,1)} %bitcast.46, bf16[64,2048]{1,0:T(8,128)(2,1)} %stream_in_ref.1, f32[1,2048]{1,0:T(1,128)} %bitcast.48, bf16[4,64,256]{2,1,0:T(8,128)(2,1)} %maximum_bitcast_fusion.maps_ref, bf16[2048,256]{1,0:T(8,128)(2,1)} %bitcast.40, bf16[2048,256]{1,0:T(8,128)(2,1)} %bitcast.42, ...), custom_call_target="tpu_custom_call" | custom-call | tf_op jit(solution)/shard_map/experts/pallas_call | solution.py:470
  107.4 1.7 %copy.55 = bf16[64,2048]{1,0:T(8,128)(2,1)} copy(bf16[64,2048]{1,0:T(8,128)(2,1)} %experts.1) | data formatting | bytes 524288
  (15 shorter events, 0.2 us)
Async XLA Ops:
  1.2 23.3 %copy-start = (bf16[128,512]{1,0:T(8,128)(2,1)S(1)}, bf16[128,512]{1,0:T(8,128)(2,1)}, u32[]{:S(2)}) copy-start(bf16[128,512]{1,0:T(8,128)(2,1)} %param.19) | copy-start | bytes 393220
  1.2 23.5 %copy-start.3 = (f32[512]{0:T(512)S(1)}, f32[512]{0:T(512)}, u32[]{:S(2)}) copy-start(f32[512]{0:T(512)} %param.22) | copy-start | bytes 6148
  25.4 11.3 %copy-start.1 = (s32[64,4]{0,1:T(4,128)S(1)}, s32[64,4]{0,1:T(4,128)}, u32[]{:S(2)}) copy-start(s32[64,4]{0,1:T(4,128)} %param.28) | copy-start | bytes 3076
  25.4 12.7 %copy-start.2 = (f32[64,4]{0,1:T(4,128)S(1)}, f32[64,4]{0,1:T(4,128)}, u32[]{:S(2)}) copy-start(f32[64,4]{0,1:T(4,128)} %param.29) | copy-start | bytes 3076
